TPU v7x, 32 devices: a whole 2x2x4 slice. The times are simulated.
32 devices in a mesh: grp: 2 (over y), sp: 4 (over z), tp: 4 (over x, core).
Axes of the slice: x: 2, y: 2, z: 4, core: 2. Of those that a mesh axis runs over, the one named last changes fastest.
Arguments:
- target: bfloat16 [1024, 2048], P(('grp', 'sp', 'tp')), parts along dimension 0, may hold values from -5 to 5
- source: bfloat16 [8192, 2048], P(('grp', 'sp', 'tp')), parts along dimension 0, may hold values from -5 to 5
- source_gain: float32 [2048], replicated, may hold values from 0.1 to 1.9
- pre_first: float32 [2048], replicated, may hold values from 0.1 to 1.9
- query_first: bfloat16 [2048, 2048], P(None, 'tp')
- keyval_first: bfloat16 [2048, 1024], P(None, 'tp')
- out_first: bfloat16 [2048, 2048], P('tp'), may hold values from -0.125 to 0.125
- post_first: float32 [2048], replicated, may hold values from 0.1 to 1.9
- ffn_pre: float32 [2048], replicated, may hold values from 0.1 to 1.9
- w_gate: bfloat16 [2048, 2816], P(None, 'tp'), may hold values from -0.125 to 0.125
- w_value: bfloat16 [2048, 2816], P(None, 'tp'), may hold values from -0.125 to 0.125
- conv_gate: float32 [3, 2816], P(None, 'tp'), may hold values from -3.5 to 3.5
- conv_value: float32 [3, 2816], P(None, 'tp'), may hold values from -3.5 to 3.5
- w_down: bfloat16 [2816, 2048], P('tp'), may hold values from -0.109375 to 0.109375
- ffn_post: float32 [2048], replicated, may hold values from 0.1 to 1.9
- pre_second: float32 [2048], replicated, may hold values from 0.1 to 1.9
- query_second: bfloat16 [2048, 2048], P(None, 'tp')
- keyval_second: bfloat16 [2048, 1024], P(None, 'tp')
- out_second: bfloat16 [2048, 2048], P('tp'), may hold values from -0.125 to 0.125
- post_second: float32 [2048], replicated, may hold values from 0.1 to 1.9
Outputs:
- decoded: float32 [1024, 2048], P(('grp', 'sp', 'tp')), parts along dimension 0
There are 2 independent parts, one for each index of `grp`. A program takes and returns all parts, laid end to end along the dimension named above; an argument that names none is the same for every part. Nothing has to cross between parts.
All inputs are finite; a program needn't handle non-finite values.
Results may differ from a plain program's by a relative error of at most 0.04.
Values may be sent and summed in bfloat16 or wider, within the bound.
No kernel may reach another device: no remote copies, remote signals or barrier semaphores. Data moves between devices by JAX's collectives and lax.ppermute only.
A program may use at most 128 MiB of HBM per device.

v0:
```python
import jax
import jax.numpy as jnp
from jax import lax
from jax.sharding import PartitionSpec as P

HEAD = 128


def swapped(block, axis, distance):
    count = lax.axis_size(axis)
    route = []
    for low in range(count):
        high = low | 1 << distance
        if high != low and high < count:
            route += [(low, high), (high, low)]
    return lax.ppermute(block, axis, route)


def shifted(value, axis, steps):
    count = lax.axis_size(axis)
    leading, last = (max(0, -steps), min(count, count - steps))
    return lax.ppermute(value, axis, [(source, source + steps) for source in range(leading, last)])


def normed(values, gain):
    widened = values.astype(jnp.float32)
    return widened * lax.rsqrt(jnp.mean(widened * widened, axis=-1, keepdims=True) + 1e-06) * gain


def project_rows(rows_here, weights):
    shard_rows = lax.all_gather(rows_here, "tp", axis=0, tiled=True)
    products = [
        jnp.dot(shard_rows, weight, preferred_element_type=jnp.float32).astype(jnp.bfloat16)
        for weight in weights
    ]
    return jnp.concatenate(products, axis=1)


def summed_rows(parts, weight):
    return lax.psum_scatter(
        jnp.dot(parts, weight, preferred_element_type=jnp.float32).astype(jnp.bfloat16),
        "tp",
        scatter_dimension=0,
        tiled=True,
    ).astype(jnp.float32)


def key_columns(source_rows, keyval_first, keyval_second):
    both_layers = jnp.concatenate([keyval_first, keyval_second], axis=1)
    columns = jnp.einsum(
        "rd,dc->cr",
        lax.all_gather(source_rows, "tp", axis=0, tiled=True),
        both_layers,
        preferred_element_type=jnp.float32,
    ).astype(jnp.bfloat16)
    column_count = keyval_first.shape[1]
    stacked = columns.reshape(2, column_count, columns.shape[1])
    own_index = lax.axis_index("tp")
    doublings = (2 * HEAD // column_count).bit_length() - 1
    for bit_number in range(doublings):
        lower_half = own_index // 2**bit_number % 2 == 0
        outgoing = stacked
        retained = stacked
        partner = swapped(outgoing, "tp", bit_number)
        stacked = jnp.where(
            lower_half,
            jnp.concatenate([retained, partner], axis=1),
            jnp.concatenate([partner, retained], axis=1),
        )
    return (stacked[:, :HEAD], stacked[:, HEAD:])


def absorber(query_heads, running, shard_pair):
    scale_factor = HEAD ** (-0.5)
    best_score, weight_sum, weighted = running
    key_block, value_block = shard_pair
    scores = (
        jnp.einsum("thd,ds->ths", query_heads, key_block, preferred_element_type=jnp.float32)
        * scale_factor
    )
    newest = jnp.max(scores, axis=2)
    rescale = jnp.exp(best_score - newest)
    weights = jnp.exp(scores - newest[:, :, None])
    weight_sum = weight_sum * rescale + jnp.sum(weights, axis=2)
    weighted = weighted * rescale[:, :, None] + jnp.einsum(
        "ths,ds->thd", weights.astype(jnp.bfloat16), value_block, preferred_element_type=jnp.float32
    )
    return (newest, weight_sum, weighted)


def empty_running(row_count, head_count):
    return (
        jnp.full((row_count, head_count), -jnp.inf, jnp.float32),
        jnp.zeros((row_count, head_count), jnp.float32),
        jnp.zeros((row_count, head_count, HEAD), jnp.float32),
    )


def attend_keys(queries, keys_t, values_t):
    row_count = queries.shape[0]
    head_count = queries.shape[1] // HEAD
    query_heads = queries.reshape(row_count, head_count, HEAD)
    best_score, weight_sum, weighted = absorber(
        query_heads,
        empty_running(row_count, head_count),
        (
            lax.all_gather(keys_t, "sp", axis=1, tiled=True),
            lax.all_gather(values_t, "sp", axis=1, tiled=True),
        ),
    )
    return (
        (weighted / weight_sum[:, :, None])
        .reshape(row_count, head_count * HEAD)
        .astype(jnp.bfloat16)
    )


def causal_mix(rim_rows, up_rows, conv_taps):
    padded = jnp.concatenate([rim_rows, up_rows], axis=0).astype(jnp.float32)
    length = up_rows.shape[0]
    return (
        conv_taps[0] * padded[:length]
        + conv_taps[1] * padded[1 : length + 1]
        + conv_taps[2] * padded[2:]
    )


def per_device(
    target,
    source,
    source_gain,
    pre_first,
    query_first,
    keyval_first,
    out_first,
    post_first,
    ffn_pre,
    w_gate,
    w_value,
    conv_gate,
    conv_value,
    w_down,
    ffn_post,
    pre_second,
    query_second,
    keyval_second,
    out_second,
    post_second,
):
    source_rows = normed(source, source_gain).astype(jnp.bfloat16)
    keys_t, values_t = key_columns(source_rows, keyval_first, keyval_second)

    def attention_layer(stream, pre_gain, w_query, layer_index, w_out, post_gain):
        queries = project_rows(normed(stream, pre_gain).astype(jnp.bfloat16), (w_query,))
        heads = attend_keys(queries, keys_t[layer_index], values_t[layer_index])
        mixed = summed_rows(heads, w_out)
        return stream.astype(jnp.float32) + normed(mixed, post_gain)

    after_first = attention_layer(target, pre_first, query_first, 0, out_first, post_first)
    up_both = project_rows(normed(after_first, ffn_pre).astype(jnp.bfloat16), (w_gate, w_value))
    hidden_width = w_gate.shape[1]
    up_gate = up_both[:, :hidden_width]
    up_value = up_both[:, hidden_width:]
    rim_gate, rim_value = shifted((up_gate[-2:], up_value[-2:]), "sp", 1)
    gated = (
        jax.nn.gelu(causal_mix(rim_gate, up_gate, conv_gate), approximate=True)
        * causal_mix(rim_value, up_value, conv_value)
    ).astype(jnp.bfloat16)
    ffn_sum = summed_rows(gated, w_down)
    after_ffn = after_first + normed(ffn_sum, ffn_post)
    return attention_layer(after_ffn, pre_second, query_second, 1, out_second, post_second)


def solution(mesh):
    placed = (
        P(("grp", "sp", "tp"), None),
        P(("grp", "sp", "tp"), None),
        P(),
        P(),
        P(None, "tp"),
        P(None, "tp"),
        P("tp", None),
        P(),
        P(),
        P(None, "tp"),
        P(None, "tp"),
        P(None, "tp"),
        P(None, "tp"),
        P("tp", None),
        P(),
        P(),
        P(None, "tp"),
        P(None, "tp"),
        P("tp", None),
        P(),
    )
    return jax.shard_map(
        per_device,
        mesh=mesh,
        in_specs=placed,
        out_specs=P(("grp", "sp", "tp"), None),
        check_vma=False,
    )
```

profile of v0, /device:TPU:0, one launch (start us, length us, event | category | flops | bytes accessed | tf_op | source)
XLA Modules:
  0.0 286.1 jit_solution(5427516378254216936)
XLA Ops:
  6.5 1.7 fusion.8
  8.2 2.5 fusion.10
  10.8 37.3 %all-gather.10.cloned.1.call-done = bf16[1024,2048]{1,0:T(8,128)(2,1)} async-done(((bf16[256,2048]{1,0:T(8,128)(2,1)}), bf16[1024,2048]{1,0:T(8,128)(2,1)}) %all-gather.10.cloned.1.call-update) | async-done | bytes 4194320 | tf_op jit(solution)/shard_map/all_gather | solution.py:52
  48.1 5.2 %fusion.15 = bf16[512,1024]{1,0:T(8,128)(2,1)S(1)} fusion(bf16[1024,2048]{1,0:T(8,128)(2,1)} %all-gather.10.cloned.1.call-done, bf16[2048,256]{1,0:T(8,128)(2,1)} %param.37, bf16[2048,256]{1,0:T(8,128)(2,1)} %param.25), kind=kOutput, calls=%fused_computation.22 | convolution fusion | flops 2152202240 | bytes 7340032 | tf_op jit(solution)/shard_map/rd,dc->cr/dot_general | solution.py:50
  55.1 7.2 %all_gather.24 = bf16[128,2048]{1,0:T(8,128)(2,1)S(1)} all-gather(bf16[32,2048]{1,0:T(8,128)(2,1)S(1)} %fusion.67), channel_id=1, replica_groups=mesh['grp'=2,'sp'=4,'tp'=4] {'tp'}, dimensions={0}, use_global_device_ids=true | all-gather | bytes 655360 | tf_op jit(solution)/shard_map/all_gather | solution.py:31
  62.3 2.1 fusion.24
  64.3 18.1 %all-gather.12.cloned.1.call-done = bf16[1,128,4096]{2,1,0:T(8,128)(2,1)} async-done(((bf16[1,128,1024]{2,1,0:T(8,128)(2,1)}), bf16[1,128,4096]{2,1,0:T(8,128)(2,1)}) %all-gather.12.cloned.1.call-update) | async-done | bytes 1048592 | tf_op jit(solution)/shard_map/all_gather | solution.py:107
  82.5 2.6 multiply_reduce_fusion.1
  85.0 1.5 fusion
  86.5 1.7 copy-done.1
  88.3 23.2 %all-gather.14.cloned.1.call-done = bf16[1,128,4096]{2,1,0:T(8,128)(2,1)} async-done(((bf16[1,128,1024]{2,1,0:T(8,128)(2,1)}), bf16[1,128,4096]{2,1,0:T(8,128)(2,1)}) %all-gather.14.cloned.1.call-update) | async-done | bytes 1048592 | tf_op jit(solution)/shard_map/all_gather | solution.py:108
  111.5 5.5 %fusion.35 = bf16[128,4,128]{0,2,1:T(8,128)(2,1)S(1)} fusion(f32[128,4,4096]{2,0,1:T(8,128)} %copy-done.1, f32[128,4]{0,1:T(4,128)S(1)} %get-tuple-element.19, bf16[1,128,4096]{2,1,0:T(8,128)(2,1)} %all-gather.14.cloned.1.call-done, f32[128,4]{0,1:T(4,128)S(1)} %get-tuple-element.18, f32[128,4]{0,1:T(4,128)S(1)} %get-tuple-element.17), kind=kOutput, calls=%fused_computation.34 | convolution fusion | flops 543358976 | bytes 9574400 | tf_op jit(solution)/shard_map/ths,ds->thd/dot_general | solution.py:85
  117.0 1.3 convolution_convert_fusion.2
  118.4 21.1 %reduce-scatter.4.cloned.1.call-done = bf16[32,2048]{1,0:T(8,128)(2,1)} async-done(((bf16[128,2048]{1,0:T(8,128)(2,1)}), bf16[32,2048]{1,0:T(8,128)(2,1)}) %reduce-scatter.4.cloned.1.call-update) | async-done | bytes 131088 | tf_op jit(solution)/shard_map/reduce_scatter | solution.py:40
  142.9 6.6 %all_gather.28 = bf16[128,2048]{1,0:T(8,128)(2,1)S(1)} all-gather(bf16[32,2048]{1,0:T(8,128)(2,1)S(1)} %multiply_convert_fusion.1), channel_id=1, replica_groups=mesh['grp'=2,'sp'=4,'tp'=4] {'tp'}, dimensions={0}, use_global_device_ids=true | all-gather | bytes 655360 | tf_op jit(solution)/shard_map/all_gather | solution.py:31
  149.5 2.7 convolution_convert_fusion.4
  152.3 3.4 %collective-permute-start = (bf16[2,704]{0,1:T(8,128)(2,1)S(1)}, bf16[2,704]{0,1:T(8,128)(2,1)S(1)}, u32[]{:S(2)}, u32[]{:S(2)}) collective-permute-start(bf16[2,704]{0,1:T(8,128)(2,1)S(1)} %slice.80), channel_id=1, source_target_pairs={{0,4},{4,8},{8,12},{1,5},{5,9},{9,13},{2,6},{6,10},{10,14},{3,7},{... | collective-permute-start | bytes 8456 | tf_op jit(solution)/shard_map/ppermute | solution.py:22
  156.8 3.6 %collective-permute-start.1 = (bf16[2,704]{0,1:T(8,128)(2,1)S(1)}, bf16[2,704]{0,1:T(8,128)(2,1)S(1)}, u32[]{:S(2)}, u32[]{:S(2)}) collective-permute-start(bf16[2,704]{0,1:T(8,128)(2,1)S(1)} %slice.84), channel_id=1, source_target_pairs={{0,4},{4,8},{8,12},{1,5},{5,9},{9,13},{2,6},{6,10},{10,14},{3,7},{... | collective-permute-start | bytes 8456 | tf_op jit(solution)/shard_map/ppermute | solution.py:22
  160.6 3.7 %collective-permute-done.1 = bf16[2,704]{0,1:T(8,128)(2,1)S(1)} collective-permute-done((bf16[2,704]{0,1:T(8,128)(2,1)S(1)}, bf16[2,704]{0,1:T(8,128)(2,1)S(1)}, u32[]{:S(2)}, u32[]{:S(2)}) %collective-permute-start.1) | collective-permute-done | bytes 2848 | tf_op jit(solution)/shard_map/ppermute | solution.py:22
  164.4 2.5 convolution_convert_fusion.1
  168.3 21.6 %reduce-scatter.6.cloned.1.call-done = bf16[32,2048]{1,0:T(8,128)(2,1)} async-done(((bf16[128,2048]{1,0:T(8,128)(2,1)}), bf16[32,2048]{1,0:T(8,128)(2,1)}) %reduce-scatter.6.cloned.1.call-update) | async-done | bytes 131088 | tf_op jit(solution)/shard_map/reduce_scatter | solution.py:40
  193.3 6.6 %all_gather.29 = bf16[128,2048]{1,0:T(8,128)(2,1)S(1)} all-gather(bf16[32,2048]{1,0:T(8,128)(2,1)S(1)} %multiply_convert_fusion), channel_id=1, replica_groups=mesh['grp'=2,'sp'=4,'tp'=4] {'tp'}, dimensions={0}, use_global_device_ids=true | all-gather | bytes 655360 | tf_op jit(solution)/shard_map/all_gather | solution.py:31
  199.9 2.0 fusion.25
  201.9 17.5 %all-gather.16.cloned.1.call-done = bf16[1,128,4096]{2,1,0:T(8,128)(2,1)} async-done(((bf16[1,128,1024]{2,1,0:T(8,128)(2,1)}), bf16[1,128,4096]{2,1,0:T(8,128)(2,1)}) %all-gather.16.cloned.1.call-update) | async-done | bytes 1048592 | tf_op jit(solution)/shard_map/all_gather | solution.py:107
  219.4 2.6 multiply_reduce_fusion
  222.0 1.5 fusion.2
  223.5 1.7 copy-done.2
  225.2 23.2 %all-gather.18.cloned.1.call-done = bf16[1,128,4096]{2,1,0:T(8,128)(2,1)} async-done(((bf16[1,128,1024]{2,1,0:T(8,128)(2,1)}), bf16[1,128,4096]{2,1,0:T(8,128)(2,1)}) %all-gather.18.cloned.1.call-update) | async-done | bytes 1048592 | tf_op jit(solution)/shard_map/all_gather | solution.py:108
  248.4 5.5 %fusion.29 = bf16[128,4,128]{0,2,1:T(8,128)(2,1)S(1)} fusion(f32[128,4,4096]{2,0,1:T(8,128)} %copy-done.2, f32[128,4]{0,1:T(4,128)S(1)} %get-tuple-element.21, bf16[1,128,4096]{2,1,0:T(8,128)(2,1)} %all-gather.18.cloned.1.call-done, f32[128,4]{0,1:T(4,128)S(1)} %get-tuple-element.16, f32[128,4]{0,1:T(4,128)S(1)} %get-tuple-element.15), kind=kOutput, calls=%fused_computation.32 | convolution fusion | flops 543358976 | bytes 9574400 | tf_op jit(solution)/shard_map/ths,ds->thd/dot_general | solution.py:85
  253.9 1.3 convolution_convert_fusion
  255.2 21.2 %reduce-scatter.8.cloned.1.call-done = bf16[32,2048]{1,0:T(8,128)(2,1)} async-done(((bf16[128,2048]{1,0:T(8,128)(2,1)}), bf16[32,2048]{1,0:T(8,128)(2,1)}) %reduce-scatter.8.cloned.1.call-update) | async-done | bytes 131088 | tf_op jit(solution)/shard_map/reduce_scatter | solution.py:40
  277.4 1.8 fusion.64
  (74 shorter events, 12.6 us)
Async XLA Ops:
  6.5 157.9 %copy-start = (bf16[704,2048]{1,0:T(8,128)(2,1)S(1)}, bf16[704,2048]{1,0:T(8,128)(2,1)}, u32[]{:S(2)}) copy-start(bf16[704,2048]{1,0:T(8,128)(2,1)} %param.33) | copy-start | bytes 8650756
  6.5 41.5 %all-gather.10.cloned.1.call-start = ((), (), s32[]{:S(2)}) async-start(), calls=%async_computation.3 | async-start | bytes 5242880 | tf_op jit(solution)/shard_map/all_gather | solution.py:52
  10.7 43.6 %copy-start.3 = (bf16[32,2048]{1,0:T(8,128)(2,1)S(1)}, bf16[32,2048]{1,0:T(8,128)(2,1)}, u32[]{:S(2)}) copy-start(bf16[32,2048]{1,0:T(8,128)(2,1)} %param.20) | copy-start | bytes 393220
  10.8 43.8 %copy-start.13 = (f32[2048]{0:T(1024)S(1)}, f32[2048]{0:T(1024)}, u32[]{:S(2)}) copy-start(f32[2048]{0:T(1024)} %param.23) | copy-start | bytes 24580
  10.8 71.7 %all-gather.12.cloned.1.call-start = ((), (), s32[]{:S(2)}) async-start(), calls=%async_computation.7 | async-start | bytes 1310720 | tf_op jit(solution)/shard_map/all_gather | solution.py:107
  54.3 57.1 %all-gather.14.cloned.1.call-start = ((), (), s32[]{:S(2)}) async-start(), calls=%async_computation.8 | async-start | bytes 1310720 | tf_op jit(solution)/shard_map/all_gather | solution.py:108
  55.1 84.4 %reduce-scatter.4.cloned.1.call-start = ((), (), s32[]{:S(2)}) async-start(), calls=%async_computation.4 | async-start | bytes 655360 | tf_op jit(solution)/shard_map/reduce_scatter | solution.py:40
  85.0 3.2 %copy-start.1 = (f32[128,4,4096]{2,0,1:T(8,128)}, f32[128,4,4096]{2,0,1:T(8,128)S(1)}, u32[]{:S(2)}) copy-start(f32[128,4,4096]{2,0,1:T(8,128)S(1)} %get-tuple-element.20) | copy-start | bytes 25165828
  111.4 5.5 %copy-start.6 = (bf16[512,2048]{1,0:T(8,128)(2,1)S(1)}, bf16[512,2048]{1,0:T(8,128)(2,1)}, u32[]{:S(2)}) copy-start(bf16[512,2048]{1,0:T(8,128)(2,1)} %param.26) | copy-start | bytes 6291460
  111.4 6.9 %copy-start.15 = (f32[3,704]{1,0:T(4,128)S(1)}, f32[3,704]{1,0:T(4,128)}, u32[]{:S(2)}) copy-start(f32[3,704]{1,0:T(4,128)} %param.32) | copy-start | bytes 25348
  111.4 6.9 %copy-start.16 = (f32[3,704]{1,0:T(4,128)S(1)}, f32[3,704]{1,0:T(4,128)}, u32[]{:S(2)}) copy-start(f32[3,704]{1,0:T(4,128)} %param.31) | copy-start | bytes 25348
  111.4 29.2 %copy-start.9 = (f32[2048]{0:T(1024)S(1)}, f32[2048]{0:T(1024)}, u32[]{:S(2)}) copy-start(f32[2048]{0:T(1024)} %param.27) | copy-start | bytes 24580
  111.4 30.4 %copy-start.14 = (f32[2048]{0:T(1024)S(1)}, f32[2048]{0:T(1024)}, u32[]{:S(2)}) copy-start(f32[2048]{0:T(1024)} %param.28) | copy-start | bytes 24580
  118.3 71.7 %reduce-scatter.6.cloned.1.call-start = ((), (), s32[]{:S(2)}) async-start(), calls=%async_computation.5 | async-start | bytes 655360 | tf_op jit(solution)/shard_map/reduce_scatter | solution.py:40
  139.5 16.3 %copy-start.5 = (bf16[2048,704]{0,1:T(8,128)(2,1)S(1)}, bf16[2048,704]{0,1:T(8,128)(2,1)}, u32[]{:S(2)}) copy-start(bf16[2048,704]{0,1:T(8,128)(2,1)} %param.30) | copy-start | bytes 8650756
  152.3 8.1 %collective-permute-start = (bf16[2,704]{0,1:T(8,128)(2,1)S(1)}, bf16[2,704]{0,1:T(8,128)(2,1)S(1)}, u32[]{:S(2)}, u32[]{:S(2)}) collective-permute-start(bf16[2,704]{0,1:T(8,128)(2,1)S(1)} %slice.80), channel_id=1, source_target_pairs={{0,4},{4,8},{8,12},{1,5},{5,9},{9,13},{2,6},{6,10},{10,14},{3,7},{... | collective-permute-start | bytes 8456 | tf_op jit(solution)/shard_map/ppermute | solution.py:22
  156.7 34.3 %copy-start.4 = (bf16[32,2048]{1,0:T(8,128)(2,1)S(1)}, bf16[32,2048]{1,0:T(8,128)(2,1)}, u32[]{:S(2)}) copy-start(bf16[32,2048]{1,0:T(8,128)(2,1)} %reduce-scatter.4.cloned.1.call-done) | copy-start | bytes 393220
  156.7 34.3 %copy-start.10 = (f32[2048]{0:T(1024)S(1)}, f32[2048]{0:T(1024)}, u32[]{:S(2)}) copy-start(f32[2048]{0:T(1024)} %param.34) | copy-start | bytes 24580
  156.7 35.5 %copy-start.11 = (f32[2048]{0:T(1024)S(1)}, f32[2048]{0:T(1024)}, u32[]{:S(2)}) copy-start(f32[2048]{0:T(1024)} %param.35) | copy-start | bytes 24580
  156.8 7.4 %collective-permute-start.1 = (bf16[2,704]{0,1:T(8,128)(2,1)S(1)}, bf16[2,704]{0,1:T(8,128)(2,1)S(1)}, u32[]{:S(2)}, u32[]{:S(2)}) collective-permute-start(bf16[2,704]{0,1:T(8,128)(2,1)S(1)} %slice.84), channel_id=1, source_target_pairs={{0,4},{4,8},{8,12},{1,5},{5,9},{9,13},{2,6},{6,10},{10,14},{3,7},{... | collective-permute-start | bytes 8456 | tf_op jit(solution)/shard_map/ppermute | solution.py:22
  166.9 52.5 %all-gather.16.cloned.1.call-start = ((), (), s32[]{:S(2)}) async-start(), calls=%async_computation.9 | async-start | bytes 1310720 | tf_op jit(solution)/shard_map/all_gather | solution.py:107
  167.5 80.8 %all-gather.18.cloned.1.call-start = ((), (), s32[]{:S(2)}) async-start(), calls=%async_computation.10 | async-start | bytes 1310720 | tf_op jit(solution)/shard_map/all_gather | solution.py:108
  168.3 108.1 %reduce-scatter.8.cloned.1.call-start = ((), (), s32[]{:S(2)}) async-start(), calls=%async_computation.6 | async-start | bytes 655360 | tf_op jit(solution)/shard_map/reduce_scatter | solution.py:40
  222.0 3.2 %copy-start.2 = (f32[128,4,4096]{2,0,1:T(8,128)}, f32[128,4,4096]{2,0,1:T(8,128)S(1)}, u32[]{:S(2)}) copy-start(f32[128,4,4096]{2,0,1:T(8,128)S(1)} %get-tuple-element.22) | copy-start | bytes 25165828
  248.4 5.5 %copy-start.7 = (bf16[512,2048]{1,0:T(8,128)(2,1)S(1)}, bf16[512,2048]{1,0:T(8,128)(2,1)}, u32[]{:S(2)}) copy-start(bf16[512,2048]{1,0:T(8,128)(2,1)} %param.38) | copy-start | bytes 6291460
  248.4 29.0 %copy-start.8 = (bf16[32,2048]{1,0:T(8,128)(2,1)S(1)}, bf16[32,2048]{1,0:T(8,128)(2,1)}, u32[]{:S(2)}) copy-start(bf16[32,2048]{1,0:T(8,128)(2,1)} %reduce-scatter.6.cloned.1.call-done) | copy-start | bytes 393220
  248.4 29.0 %copy-start.12 = (f32[2048]{0:T(1024)S(1)}, f32[2048]{0:T(1024)}, u32[]{:S(2)}) copy-start(f32[2048]{0:T(1024)} %param.39) | copy-start | bytes 24580
Sparse Core Ops, SparseCore 0:
  10.9 37.1 all-gather.9
  54.4 27.9 all-gather.11
  84.0 27.3 all-gather.13
  118.4 21.0 reduce-scatter.3
  167.1 22.8 reduce-scatter.5
  191.4 27.9 all-gather.15
  221.0 27.3 all-gather.17
  255.3 20.9 reduce-scatter.7
where the time goes:
time: 287 us; the launch traced here: 286 us
  waiting for transfers between devices  188 us (66%)
  matrix products  34.1 us (12%)
  blocking collectives  20.4 us (7%)
  other arithmetic  17.4 us (6%)
  between operations  13.8 us (5%)
  starting transfers between devices  7.26 us (3%)
  local copies, waits for them, and re-layouts  4.77 us (2%)
    reduce_scatter x3, waiting for transfers between devices, summed_rows(): lax.psum_scatter(jnp.dot(parts, weight, preferred_element_type=jnp.float3...  63.8 us
    all_gather x2, waiting for transfers between devices, attend_keys(): lax.all_gather(values_t, 'sp', axis=1, tiled=True)  46.3 us
    all_gather x1, waiting for transfers between devices, key_columns(): lax.all_gather(source_rows, 'tp', axis=0, tiled=True)  37.3 us
    all_gather x2, waiting for transfers between devices, attend_keys(): lax.all_gather(keys_t, 'sp', axis=1, tiled=True)  35.6 us
    all_gather x3, blocking collectives, project_rows(): shard_rows = lax.all_gather(rows_here, 'tp', axis=0, tiled=True)  20.4 us
    dot_general x2, matrix products, absorber(): jnp.einsum('ths,ds->thd', weights.astype(jnp.bfloat16), value_block, pref...  11 us
    dot_general x4, matrix products, project_rows(): jnp.dot(shard_rows, weight, preferred_element_type=jnp.float32)  7.73 us
    reduce_sum x7, other arithmetic, normed(): jnp.mean(widened * widened, axis=-1, keepdims=True) + 1e-06  7.38 us
  transfers between devices with their start and end apart: 10, of which 9 were waited for; matrix products, arithmetic and copies ran while one was open for 6% of the time, Pallas kernels for 0%

commit v1 on v0

--- a/solution.py
+++ b/solution.py
@@ -1,6 +1,10 @@
+import functools
+
 import jax
 import jax.numpy as jnp
 from jax import lax
+from jax.experimental import pallas as pl
+from jax.experimental.pallas import tpu as pltpu
 from jax.sharding import PartitionSpec as P
 
 HEAD = 128
@@ -171,6 +175,355 @@
     return attention_layer(after_ffn, pre_second, query_second, 1, out_second, post_second)
 
 
+def swapped_mask(block, axis, mask):
+    count = lax.axis_size(axis)
+    return lax.ppermute(block, axis, [(index, index ^ mask) for index in range(count)])
+
+
+def launch(body, outs, *operands, scratch=(), limit=24):
+    return pl.pallas_call(
+        body,
+        out_shape=outs,
+        scratch_shapes=list(scratch),
+        compiler_params=pltpu.CompilerParams(vmem_limit_bytes=limit << 20),
+    )(*operands)
+
+
+def dot32(left, right):
+    return jnp.dot(left, right, preferred_element_type=jnp.float32)
+
+
+def dot_nt(left, right):
+    return lax.dot_general(
+        left, right, (((1,), (1,)), ((), ())), preferred_element_type=jnp.float32
+    )
+
+
+def query_body(top_ref, low_ref, gain_ref, weight_ref, out_ref):
+    half = top_ref.shape[0]
+    for index, ref in enumerate((top_ref, low_ref)):
+        hidden = normed(ref[...], gain_ref[...]).astype(jnp.bfloat16)
+        out_ref[index * half : (index + 1) * half] = dot32(hidden, weight_ref[...]).astype(
+            jnp.bfloat16
+        )
+
+
+def keyval_body(*refs):
+    *row_refs, gain_ref, weight_ref, rows_out, keyval_out = refs
+    start = 0
+    for ref in row_refs:
+        stop = start + ref.shape[0]
+        rows_out[start:stop] = normed(ref[...], gain_ref[...]).astype(jnp.bfloat16)
+        start = stop
+    keyval_out[...] = dot32(rows_out[...], weight_ref[...]).astype(jnp.bfloat16)
+
+
+def project_body(*refs):
+    *row_refs, weight_ref, out_ref = refs
+    start = 0
+    for ref in row_refs:
+        stop = start + ref.shape[0]
+        out_ref[start:stop] = dot32(ref[...], weight_ref[...]).astype(jnp.bfloat16)
+        start = stop
+
+
+EXPONENT_SCALE = HEAD ** (-0.5) * 1.4426950408889634
+
+
+def head_partial(query, keyval_refs):
+    scores = [dot_nt(query, ref[:, :HEAD]) for ref in keyval_refs]
+    best = functools.reduce(
+        jnp.maximum, [jnp.max(block, axis=1, keepdims=True) for block in scores]
+    )
+    weight_sum, weighted = 0.0, 0.0
+    for block, ref in zip(scores, keyval_refs):
+        weights = jnp.exp2((block - best) * EXPONENT_SCALE)
+        weight_sum += jnp.sum(weights, axis=1, keepdims=True)
+        weighted += dot32(weights.astype(jnp.bfloat16), ref[:, HEAD:])
+    return best, weight_sum, weighted
+
+
+STAT_ROWS = 16
+
+
+def partial_body(query_ref, *refs):
+    *keyval_refs, out_ref = refs
+    rows, width = query_ref.shape
+    lane = lax.broadcasted_iota(jnp.int32, (rows, HEAD), 1)
+    levels = jnp.zeros((rows, HEAD), jnp.float32)
+    for head in range(width // HEAD):
+        columns = slice(head * HEAD, (head + 1) * HEAD)
+        best, weight_sum, weighted = head_partial(query_ref[:, columns], keyval_refs)
+        out_ref[:rows, columns] = (weighted / weight_sum).astype(jnp.bfloat16)
+        level = best * EXPONENT_SCALE + jnp.log2(weight_sum)
+        levels = jnp.where(lane == head, level, levels)
+    left = levels.T[:STAT_ROWS]
+    for piece in range(3):
+        rounded = left.astype(jnp.bfloat16)
+        out_ref[rows:, piece * rows : (piece + 1) * rows] = rounded
+        left = left - rounded.astype(jnp.float32)
+
+
+def joined_heads(partial_refs, heads_ref):
+    rows, width = heads_ref.shape
+    levels = [
+        sum(
+            ref[rows:, piece * rows : (piece + 1) * rows].astype(jnp.float32) for piece in range(3)
+        )
+        for ref in partial_refs
+    ]
+    best = functools.reduce(jnp.maximum, levels)
+    shares = [jnp.exp2(level - best) for level in levels]
+    total = functools.reduce(jnp.add, shares)
+    filler = jnp.zeros((HEAD - STAT_ROWS, rows), jnp.float32)
+    columns = [jnp.concatenate([share / total, filler], axis=0).T for share in shares]
+    for head in range(width // HEAD):
+        part = slice(head * HEAD, (head + 1) * HEAD)
+        heads_ref[:, part] = sum(
+            ref[:rows, part].astype(jnp.float32) * column[:, head : head + 1]
+            for ref, column in zip(partial_refs, columns)
+        ).astype(jnp.bfloat16)
+
+
+def join_out_body(*refs):
+    *partial_refs, weight_ref, keep_ref, send_ref, heads_ref = refs
+    joined_heads(partial_refs, heads_ref)
+    half = keep_ref.shape[0]
+    send_ref[...] = dot32(heads_ref[half:], weight_ref[...]).astype(jnp.bfloat16)
+    keep_ref[...] = dot32(heads_ref[:half], weight_ref[...]).astype(jnp.bfloat16)
+
+
+def residual_body(own_ref, other_ref, stream_ref, post_ref, pre_ref, stream_out, hidden_out):
+    quarter = own_ref.shape[0] // 2
+    for index in range(2):
+        here = slice(index * quarter, (index + 1) * quarter)
+        there = slice((1 - index) * quarter, (2 - index) * quarter)
+        mixed = own_ref[here].astype(jnp.float32) + other_ref[there].astype(jnp.float32)
+        stream = stream_ref[here].astype(jnp.float32) + normed(mixed, post_ref[...])
+        stream_out[here] = stream
+        hidden_out[here] = normed(stream, pre_ref[...]).astype(jnp.bfloat16)
+
+
+def last_body(own_ref, other_ref, stream_ref, post_ref, out_ref):
+    mixed = own_ref[...].astype(jnp.float32) + other_ref[...].astype(jnp.float32)
+    out_ref[...] = stream_ref[...] + normed(mixed, post_ref[...])
+
+
+LOCAL_ORDER = (0, 2, 1, 3)
+
+
+def up_body(own_ref, other_ref, gate_ref, value_ref, gate_out, value_out):
+    quarter = own_ref.shape[0] // 2
+    place = lax.axis_index("tp")
+    rows = jnp.concatenate([own_ref[...], other_ref[...]], axis=0)
+    for weight_ref, out_ref in ((gate_ref, gate_out), (value_ref, value_out)):
+        product = dot32(rows, weight_ref[...]).astype(jnp.bfloat16)
+        for index, mask in enumerate(LOCAL_ORDER):
+            where = pl.multiple_of((place ^ mask) * quarter, quarter)
+            out_ref[pl.ds(where, quarter)] = product[index * quarter : (index + 1) * quarter]
+
+
+def mixed_taps(rim_ref, up_ref, taps_ref):
+    ups = jnp.concatenate(
+        [rim_ref[...].astype(jnp.float32), up_ref[...].astype(jnp.float32)], axis=0
+    )
+    rim, rows = rim_ref.shape[0], up_ref.shape[0]
+    return sum(
+        taps_ref[tap : tap + 1] * ups[rim - 2 + tap : rim - 2 + tap + rows] for tap in range(3)
+    )
+
+
+def down_body(
+    rim_gate, up_gate, conv_gate, rim_value, up_value, conv_value, down_ref, keep_ref, send_ref, gated_ref
+):
+    gated_ref[...] = (
+        jax.nn.gelu(mixed_taps(rim_gate, up_gate, conv_gate), approximate=True)
+        * mixed_taps(rim_value, up_value, conv_value)
+    ).astype(jnp.bfloat16)
+    quarter = keep_ref.shape[0] // 2
+    place = lax.axis_index("tp")
+    for ref, masks in ((send_ref, LOCAL_ORDER[2:]), (keep_ref, LOCAL_ORDER[:2])):
+        rows = jnp.concatenate(
+            [
+                gated_ref[pl.ds(pl.multiple_of((place ^ mask) * quarter, quarter), quarter)]
+                for mask in masks
+            ],
+            axis=0,
+        )
+        ref[...] = dot32(rows, down_ref[...]).astype(jnp.bfloat16)
+
+
+def second_body(*refs):
+    own_ref, other_ref, query_ref, *keyval_refs, weight_ref, keep_ref, send_ref, queries_ref, heads_ref = refs
+    half = own_ref.shape[0]
+    queries_ref[:half] = dot32(own_ref[...], query_ref[...]).astype(jnp.bfloat16)
+    queries_ref[half:] = dot32(other_ref[...], query_ref[...]).astype(jnp.bfloat16)
+    for head in range(heads_ref.shape[1] // HEAD):
+        columns = slice(head * HEAD, (head + 1) * HEAD)
+        best, weight_sum, weighted = head_partial(queries_ref[:, columns], keyval_refs)
+        heads_ref[:, columns] = (weighted / weight_sum).astype(jnp.bfloat16)
+    send_ref[...] = dot32(heads_ref[half:], weight_ref[...]).astype(jnp.bfloat16)
+    keep_ref[...] = dot32(heads_ref[:half], weight_ref[...]).astype(jnp.bfloat16)
+
+
+def shape_of(rows, columns, dtype=jnp.bfloat16):
+    return jax.ShapeDtypeStruct((rows, columns), dtype)
+
+
+CHUNKS = 4
+
+
+def per_device_paired(
+    target,
+    source,
+    source_gain,
+    pre_first,
+    query_first,
+    keyval_first,
+    out_first,
+    post_first,
+    ffn_pre,
+    w_gate,
+    w_value,
+    conv_gate,
+    conv_value,
+    w_down,
+    ffn_post,
+    pre_second,
+    query_second,
+    keyval_second,
+    out_second,
+    post_second,
+):
+    quarter, width = target.shape
+    half, rows = 2 * quarter, 4 * quarter
+    head_width, keyval_width, hidden_width = query_first.shape[1], keyval_first.shape[1], w_gate.shape[1]
+    sp_count = lax.axis_size("sp")
+    row = lambda gain: gain.reshape(1, -1)
+
+    own_target = jnp.concatenate([target, swapped_mask(target, "tp", 2)], axis=0)
+    other_target = swapped_mask(own_target, "tp", 1)
+    queries = launch(
+        query_body, shape_of(rows, head_width), own_target, other_target, row(pre_first), query_first
+    )
+    query_blocks = [queries] + [swapped_mask(queries, "sp", mask) for mask in range(1, sp_count)]
+
+    span = source.shape[0] // CHUNKS
+    normed_rows, keyvals_first = [], []
+    for chunk in range(CHUNKS):
+        here = source[chunk * span : (chunk + 1) * span]
+        across = swapped_mask(here, "tp", 2)
+        pieces = (here, swapped_mask(here, "tp", 1), across, swapped_mask(across, "tp", 1))
+        chunk_rows, chunk_keyval = launch(
+            keyval_body,
+            (shape_of(4 * span, width), shape_of(4 * span, keyval_width)),
+            *pieces,
+            row(source_gain),
+            keyval_first,
+        )
+        normed_rows.append(chunk_rows)
+        keyvals_first.append(chunk_keyval)
+    keyval_here = launch(
+        project_body, shape_of(4 * source.shape[0], keyval_width), *normed_rows, keyval_second
+    )
+
+    packed = shape_of(rows + STAT_ROWS, head_width)
+    partials = [None] * sp_count
+    for mask in (3, 2, 1, 0) if sp_count == 4 else range(sp_count - 1, -1, -1):
+        partial = launch(partial_body, packed, query_blocks[mask], *keyvals_first)
+        partials[mask] = swapped_mask(partial, "sp", mask) if mask else partial
+    halves = (shape_of(half, width), shape_of(half, width))
+
+    def pair_sum(keep, send):
+        received = swapped_mask(send, "tp", 1)
+        return (keep.astype(jnp.float32) + received.astype(jnp.float32)).astype(jnp.bfloat16)
+
+    def residual(own, stream, post_gain, pre_gain):
+        other = swapped_mask(own, "tp", 2)
+        stream, hidden = launch(
+            residual_body,
+            (shape_of(half, width, jnp.float32), shape_of(half, width)),
+            own,
+            other,
+            stream,
+            row(post_gain),
+            row(pre_gain),
+        )
+        return stream, hidden, swapped_mask(hidden, "tp", 1)
+
+    keep, send = launch(
+        join_out_body,
+        halves,
+        *partials,
+        out_first,
+        scratch=[pltpu.VMEM((rows, head_width), jnp.bfloat16)],
+    )
+    own = pair_sum(keep, send)
+
+    keyval_here, own = lax.optimization_barrier((keyval_here, own))
+    keyvals_second = [keyval_here]
+    for bit in reversed(range((sp_count - 1).bit_length())):
+        keyvals_second += [swapped_mask(part, "sp", 1 << bit) for part in keyvals_second]
+
+    after_first, hidden, other_hidden = residual(own, own_target, post_first, ffn_pre)
+    up_gate, up_value = launch(
+        up_body,
+        (shape_of(rows, hidden_width), shape_of(rows, hidden_width)),
+        hidden,
+        other_hidden,
+        w_gate,
+        w_value,
+    )
+    rim = jnp.concatenate([up_gate[-8:], up_value[-8:]], axis=0)
+    rim = shifted(rim, "sp", 1)
+    keep, send = launch(
+        down_body,
+        halves,
+        rim[:8],
+        up_gate,
+        conv_gate,
+        rim[8:],
+        up_value,
+        conv_value,
+        w_down,
+        scratch=[pltpu.VMEM((rows, hidden_width), jnp.bfloat16)],
+    )
+    after_ffn, hidden, other_hidden = residual(pair_sum(keep, send), after_first, ffn_post, pre_second)
+    keep, send = launch(
+        second_body,
+        halves,
+        hidden,
+        other_hidden,
+        query_second,
+        *keyvals_second,
+        out_second,
+        scratch=[pltpu.VMEM((rows, head_width), jnp.bfloat16)] * 2,
+        limit=32,
+    )
+    own = pair_sum(keep, send)
+    return launch(
+        last_body,
+        shape_of(quarter, width, jnp.float32),
+        own[:quarter],
+        swapped_mask(own[quarter:], "tp", 2),
+        after_ffn[:quarter],
+        row(post_second),
+    )
+
+
+def chosen(*arrays):
+    target, keyval_first, query_first = arrays[0], arrays[5], arrays[4]
+    sp_count = lax.axis_size("sp")
+    fits = (
+        lax.axis_size("tp") == 4
+        and sp_count & (sp_count - 1) == 0
+        and 4 * target.shape[0] == HEAD
+        and keyval_first.shape[1] == 2 * HEAD
+        and 3 * HEAD <= query_first.shape[1] <= STAT_ROWS * HEAD
+    )
+    return (per_device_paired if fits else per_device)(*arrays)
+
+
 def solution(mesh):
     placed = (
         P(("grp", "sp", "tp"), None),
@@ -195,7 +548,7 @@
         P(),
     )
     return jax.shard_map(
-        per_device,
+        chosen,
         mesh=mesh,
         in_specs=placed,
         out_specs=P(("grp", "sp", "tp"), None),

time: 287 us -> 149 us (0.52)
  waiting for transfers between devices: 188 us -> 77.9 us
  matrix products: 34.1 us -> 0 us
  starting transfers between devices: 7.26 us -> 32.8 us
  Pallas kernels: 0 us -> 23.8 us
  blocking collectives: 20.4 us -> 0 us
  other arithmetic: 17.4 us -> 0.2 us
  between operations: 13.8 us -> 0.41 us
  local copies, waits for them, and re-layouts: 4.77 us -> 13.6 us
    all_gather x5 -> x0, waiting for transfers between devices: 119 us -> none  [the longest x2 46.3 us: attend_keys(): lax.all_gather(values_t, 'sp', axis=1, tiled=True)]
    ppermute x0 -> x31, waiting for transfers between devices: none -> 76.4 us  [swapped_mask(): lax.ppermute(block, axis, [(index, index ^ mask) for index in range(count)])]
    reduce_scatter x3 -> x0, waiting for transfers between devices: 63.8 us -> none  [summed_rows(): lax.psum_scatter(jnp.dot(parts, weight, preferred_element_type=jnp.float3...]
    dot_general x12 -> x0, matrix products: 34.1 us -> none  [the longest x2 11 us: absorber(): jnp.einsum('ths,ds->thd', weights.astype(jnp.bfloat16), value_block, pref...]
    ppermute x0 -> x31, starting transfers between devices: none -> 29.3 us  [swapped_mask(): lax.ppermute(block, axis, [(index, index ^ mask) for index in range(count)])]
    pallas_call x0 -> x17, Pallas kernels: none -> 23.8 us  [launch(): pl.pallas_call(body, out_shape=outs, scratch_shapes=list(scratch), compil...]
    all_gather x3 -> x0, blocking collectives: 20.4 us -> none  [project_rows(): shard_rows = lax.all_gather(rows_here, 'tp', axis=0, tiled=True)]
    reduce_sum x9 -> x0, other arithmetic: 10.4 us -> none  [the longest x7 7.38 us: normed(): jnp.mean(widened * widened, axis=-1, keepdims=True) + 1e-06]
  transfers between devices with their start and end apart: 10 -> 32, of which waited for: 9 -> 14; matrix products, arithmetic and copies ran while one was open for 6% -> 6% of each run, Pallas kernels for 0% -> 8%
where the time goes in v1:
time: 149 us
  waiting for transfers between devices  77.9 us (52%)
  starting transfers between devices  32.8 us (22%)
  Pallas kernels  23.8 us (16%)
  local copies, waits for them, and re-layouts  13.6 us (9%)
    ppermute x31, waiting for transfers between devices, swapped_mask(): lax.ppermute(block, axis, [(index, index ^ mask) for index in range(count)])  76.4 us
    ppermute x31, starting transfers between devices, swapped_mask(): lax.ppermute(block, axis, [(index, index ^ mask) for index in range(count)])  29.3 us
    pallas_call x17, Pallas kernels, launch(): pl.pallas_call(body, out_shape=outs, scratch_shapes=list(scratch), compil...  23.8 us
    unnamed x45, local copies, waits for them, and re-layouts  12.2 us
    ppermute x1, starting transfers between devices, shifted(): lax.ppermute(value, axis, [(source, source + steps) for source in range(l...  3.44 us
  transfers between devices with their start and end apart: 32, of which 14 were waited for; matrix products, arithmetic and copies ran while one was open for 6% of the time, Pallas kernels for 8%

profile of v1, /device:TPU:0, one launch (start us, length us, event | category | flops | bytes accessed | tf_op | source)
XLA Modules:
  0.0 148.8 jit_solution(4538166305763015222)
XLA Ops:
  1.4 3.0 %collective-permute-start.7 = (bf16[64,2048]{1,0:T(8,128)(2,1)S(1)}, bf16[64,2048]{1,0:T(8,128)(2,1)S(1)}, u32[]{:S(2)}, u32[]{:S(2)}) collective-permute-start(bf16[64,2048]{1,0:T(8,128)(2,1)S(1)} %get-tuple-element.52.refs_0_), channel_id=1, source_target_pairs={{0,2},{1,3},{2,0},{3,1},{4,6},{5,7},{6,4},{7,5},{8,10},{9,11},{10,... | collective-permute-start | bytes 786440 | tf_op jit(solution)/shard_map/ppermute | solution.py:180
  5.0 1.7 %collective-permute-start.12 = (bf16[32,2048]{1,0:T(8,128)(2,1)}, bf16[32,2048]{1,0:T(8,128)(2,1)S(1)}, u32[]{:S(2)}, u32[]{:S(2)}) collective-permute-start(bf16[32,2048]{1,0:T(8,128)(2,1)} %param.20), channel_id=1, source_target_pairs={{0,2},{1,3},{2,0},{3,1},{4,6},{5,7},{6,4},{7,5},{8,10},{9,11},{10,... | collective-permute-start | bytes 393224 | tf_op jit(solution)/shard_map/ppermute | solution.py:180
  7.7 11.5 %collective-permute-done.12 = bf16[32,2048]{1,0:T(8,128)(2,1)S(1)} collective-permute-done((bf16[32,2048]{1,0:T(8,128)(2,1)}, bf16[32,2048]{1,0:T(8,128)(2,1)S(1)}, u32[]{:S(2)}, u32[]{:S(2)}) %collective-permute-start.12) | collective-permute-done | bytes 131104 | tf_op jit(solution)/shard_map/ppermute | solution.py:180
  19.2 1.7 %collective-permute-start.4 = (bf16[64,2048]{1,0:T(8,128)(2,1)S(1)}, bf16[64,2048]{1,0:T(8,128)(2,1)S(1)}, u32[]{:S(2)}, u32[]{:S(2)}) collective-permute-start(bf16[64,2048]{1,0:T(8,128)(2,1)S(1)} %get-tuple-element.50.refs_0_), channel_id=1, source_target_pairs={{0,2},{1,3},{2,0},{3,1},{4,6},{5,7},{6,4},{7,5},{8,10},{9,11},{10,... | collective-permute-start | bytes 786440 | tf_op jit(solution)/shard_map/ppermute | solution.py:180
  21.8 6.5 %collective-permute-done.4.refs_2_ = bf16[64,2048]{1,0:T(8,128)(2,1)S(1)} collective-permute-done((bf16[64,2048]{1,0:T(8,128)(2,1)S(1)}, bf16[64,2048]{1,0:T(8,128)(2,1)S(1)}, u32[]{:S(2)}, u32[]{:S(2)}) %collective-permute-start.4) | collective-permute-done | bytes 262176 | tf_op jit(solution)/shard_map/ppermute | solution.py:180
  28.9 3.4 %collective-permute-done.1.refs_2_ = bf16[64,2048]{1,0:T(8,128)(2,1)S(1)} collective-permute-done((bf16[64,2048]{1,0:T(8,128)(2,1)S(1)}, bf16[64,2048]{1,0:T(8,128)(2,1)S(1)}, u32[]{:S(2)}, u32[]{:S(2)}) %collective-permute-start.1) | collective-permute-done | bytes 262176 | tf_op jit(solution)/shard_map/ppermute | solution.py:180
  34.4 3.6 %collective-permute-start.18 = (bf16[128,512]{1,0:T(8,128)(2,1)S(1)}, bf16[128,512]{1,0:T(8,128)(2,1)S(1)}, u32[]{:S(2)}, u32[]{:S(2)}) collective-permute-start(bf16[128,512]{1,0:T(8,128)(2,1)S(1)} %shard_map.195.query_ref), channel_id=1, source_target_pairs={{0,12},{4,8},{8,4},{12,0},{1,13},{5,9},{9,5},{13,1},{2,14},{6,10},... | collective-permute-start | bytes 393224 | tf_op jit(solution)/shard_map/ppermute | solution.py:180
  42.8 1.6 %shard_map.199 = bf16[144,512]{1,0:T(8,128)(2,1)S(1)} custom-call(bf16[128,512]{1,0:T(8,128)(2,1)S(1)} %collective-permute-done.18.query_ref, bf16[256,256]{1,0:T(8,128)(2,1)S(1)} %get-tuple-element.31.refs_0_, bf16[256,256]{1,0:T(8,128)(2,1)S(1)} %get-tuple-element.32.refs_1_, bf16[256,256]{1,0:T(8,128)(2,1)S(1)} %get-tuple-element.33.refs_2_, ...), custom_call_target="tpu_custom_call" | custom-call | tf_op jit(solution)/shard_map/pallas_call | solution.py:184
  44.3 3.7 %collective-permute-start.19 = (bf16[144,512]{1,0:T(8,128)(2,1)S(1)}, bf16[144,512]{1,0:T(8,128)(2,1)S(1)}, u32[]{:S(2)}, u32[]{:S(2)}) collective-permute-start(bf16[144,512]{1,0:T(8,128)(2,1)S(1)} %shard_map.199), channel_id=1, source_target_pairs={{0,12},{4,8},{8,4},{12,0},{1,13},{5,9},{9,5},{13,1},{2,14},{6,10},... | collective-permute-start | bytes 442376 | tf_op jit(solution)/shard_map/ppermute | solution.py:180
  48.0 5.4 %collective-permute-done.16.query_ref = bf16[128,512]{1,0:T(8,128)(2,1)S(1)} collective-permute-done((bf16[128,512]{1,0:T(8,128)(2,1)S(1)}, bf16[128,512]{1,0:T(8,128)(2,1)S(1)}, u32[]{:S(2)}, u32[]{:S(2)}) %collective-permute-start.16) | collective-permute-done | bytes 131104 | tf_op jit(solution)/shard_map/ppermute | solution.py:180
  53.4 1.6 %shard_map.198 = bf16[144,512]{1,0:T(8,128)(2,1)S(1)} custom-call(bf16[128,512]{1,0:T(8,128)(2,1)S(1)} %collective-permute-done.16.query_ref, bf16[256,256]{1,0:T(8,128)(2,1)S(1)} %get-tuple-element.31.refs_0_, bf16[256,256]{1,0:T(8,128)(2,1)S(1)} %get-tuple-element.32.refs_1_, bf16[256,256]{1,0:T(8,128)(2,1)S(1)} %get-tuple-element.33.refs_2_, ...), custom_call_target="tpu_custom_call" | custom-call | tf_op jit(solution)/shard_map/pallas_call | solution.py:184
  55.1 1.6 %shard_map.197 = bf16[144,512]{1,0:T(8,128)(2,1)S(1)} custom-call(bf16[128,512]{1,0:T(8,128)(2,1)S(1)} %collective-permute-done.14.query_ref, bf16[256,256]{1,0:T(8,128)(2,1)S(1)} %get-tuple-element.31.refs_0_, bf16[256,256]{1,0:T(8,128)(2,1)S(1)} %get-tuple-element.32.refs_1_, bf16[256,256]{1,0:T(8,128)(2,1)S(1)} %get-tuple-element.33.refs_2_, ...), custom_call_target="tpu_custom_call" | custom-call | tf_op jit(solution)/shard_map/pallas_call | solution.py:184
  56.6 3.1 %collective-permute-start.15 = (bf16[144,512]{1,0:T(8,128)(2,1)S(1)}, bf16[144,512]{1,0:T(8,128)(2,1)S(1)}, u32[]{:S(2)}, u32[]{:S(2)}) collective-permute-start(bf16[144,512]{1,0:T(8,128)(2,1)S(1)} %shard_map.197), channel_id=1, source_target_pairs={{0,4},{4,0},{8,12},{12,8},{1,5},{5,1},{9,13},{13,9},{2,6},{6,2},{1... | collective-permute-start | bytes 442376 | tf_op jit(solution)/shard_map/ppermute | solution.py:180
  59.7 1.6 %shard_map.196.refs_0_ = bf16[144,512]{1,0:T(8,128)(2,1)S(1)} custom-call(bf16[128,512]{1,0:T(8,128)(2,1)S(1)} %shard_map.195.query_ref, bf16[256,256]{1,0:T(8,128)(2,1)S(1)} %get-tuple-element.31.refs_0_, bf16[256,256]{1,0:T(8,128)(2,1)S(1)} %get-tuple-element.32.refs_1_, bf16[256,256]{1,0:T(8,128)(2,1)S(1)} %get-tuple-element.33.refs_2_, ...), custom_call_target="tpu_custom_call" | custom-call | tf_op jit(solution)/shard_map/pallas_call | solution.py:184
  66.4 1.6 %collective-permute-start.21 = (bf16[64,2048]{1,0:T(8,128)(2,1)S(1)}, bf16[64,2048]{1,0:T(8,128)(2,1)S(1)}, u32[]{:S(2)}, u32[]{:S(2)}) collective-permute-start(bf16[64,2048]{1,0:T(8,128)(2,1)S(1)} %add_convert_fusion.2.own_ref), channel_id=1, source_target_pairs={{0,2},{1,3},{2,0},{3,1},{4,6},{5,7},{6,4},{7,5},{8,10},{9,11},{10,... | collective-permute-start | bytes 786440 | tf_op jit(solution)/shard_map/ppermute | solution.py:180
  68.0 7.0 %collective-permute-done.21.other_ref = bf16[64,2048]{1,0:T(8,128)(2,1)S(1)} collective-permute-done((bf16[64,2048]{1,0:T(8,128)(2,1)S(1)}, bf16[64,2048]{1,0:T(8,128)(2,1)S(1)}, u32[]{:S(2)}, u32[]{:S(2)}) %collective-permute-start.21) | collective-permute-done | bytes 262176 | tf_op jit(solution)/shard_map/ppermute | solution.py:180
  76.3 3.1 %copy.21.gate_ref = bf16[2048,704]{1,0:T(8,128)(2,1)S(1)} copy(bf16[2048,704]{0,1:T(8,128)(2,1)} %param.29) | data formatting | bytes 5767168 | tf_op args[9]
  79.4 4.6 %copy.22.value_ref = bf16[2048,704]{1,0:T(8,128)(2,1)} copy(bf16[2048,704]{0,1:T(8,128)(2,1)} %param.30) | data formatting | bytes 5767168 | tf_op args[10]
  84.1 1.9 %copy-done.1 = bf16[2048,704]{1,0:T(8,128)(2,1)S(1)} copy-done((bf16[2048,704]{1,0:T(8,128)(2,1)S(1)}, bf16[2048,704]{1,0:T(8,128)(2,1)}, u32[]{:S(2)}) %copy-start.1) | copy-done | bytes 2883608
  86.0 2.1 %shard_map.202 = (bf16[128,704]{1,0:T(8,128)(2,1)S(1)}, bf16[128,704]{1,0:T(8,128)(2,1)S(1)}) custom-call(bf16[64,2048]{1,0:T(8,128)(2,1)S(1)} %get-tuple-element.38.own_ref, bf16[64,2048]{1,0:T(8,128)(2,1)} %collective-permute-done.22.other_ref, bf16[2048,704]{1,0:T(8,128)(2,1)S(1)} %copy.21.gate_ref, bf16[2048,704]{1,0:T(8,128)(2,1)S(1)} %copy-done.1), custom_call_target="tpu_custom_call" | custom-call | tf_op jit(solution)/shard_map/pallas_call | solution.py:184
  88.2 3.4 %collective-permute-start.23 = (bf16[16,704]{1,0:T(8,128)(2,1)S(1)}, bf16[16,704]{1,0:T(8,128)(2,1)S(1)}, u32[]{:S(2)}, u32[]{:S(2)}) collective-permute-start(bf16[16,704]{1,0:T(8,128)(2,1)S(1)} %pad_maximum_fusion), channel_id=1, source_target_pairs={{0,4},{4,8},{8,12},{1,5},{5,9},{9,13},{2,6},{6,10},{10,14},{3,7},{... | collective-permute-start | bytes 67592 | tf_op jit(solution)/shard_map/ppermute | solution.py:26
  91.7 1.5 %collective-permute-done.23 = bf16[16,704]{1,0:T(8,128)(2,1)S(1)} collective-permute-done((bf16[16,704]{1,0:T(8,128)(2,1)S(1)}, bf16[16,704]{1,0:T(8,128)(2,1)S(1)}, u32[]{:S(2)}, u32[]{:S(2)}) %collective-permute-start.23) | collective-permute-done | bytes 22560 | tf_op jit(solution)/shard_map/ppermute | solution.py:26
  93.2 1.8 %shard_map.203 = (bf16[64,2048]{1,0:T(8,128)(2,1)S(1)}, bf16[64,2048]{1,0:T(8,128)(2,1)S(1)}) custom-call(bf16[8,704]{1,0:T(8,128)(2,1)S(1)} %get-tuple-element.56.rim_gate, bf16[128,704]{1,0:T(8,128)(2,1)S(1)} %get-tuple-element.39.up_gate, f32[3,704]{1,0:T(4,128)S(1)} %copy-done.13, bf16[8,704]{1,0:T(8,128)(2,1)S(1)} %get-tuple-element.55.rim_value, ...), custom_call_target="tpu_custom_call" | custom-call | tf_op jit(solution)/shard_map/pallas_call | solution.py:184
  95.1 2.3 %collective-permute-start.27 = (bf16[1024,256]{1,0:T(8,128)(2,1)S(1)}, bf16[1024,256]{1,0:T(8,128)(2,1)S(1)}, u32[]{:S(2)}, u32[]{:S(2)}) collective-permute-start(bf16[1024,256]{1,0:T(8,128)(2,1)S(1)} %copy-done.8), channel_id=1, source_target_pairs={{0,8},{4,12},{8,0},{12,4},{1,9},{5,13},{9,1},{13,5},{2,10},{6,14},... | collective-permute-start | bytes 1572872 | tf_op jit(solution)/shard_map/ppermute | solution.py:180
  97.4 1.6 %collective-permute-start.25 = (bf16[64,2048]{1,0:T(8,128)(2,1)S(1)}, bf16[64,2048]{1,0:T(8,128)(2,1)S(1)}, u32[]{:S(2)}, u32[]{:S(2)}) collective-permute-start(bf16[64,2048]{1,0:T(8,128)(2,1)S(1)} %add_convert_fusion.1.own_ref), channel_id=1, source_target_pairs={{0,2},{1,3},{2,0},{3,1},{4,6},{5,7},{6,4},{7,5},{8,10},{9,11},{10,... | collective-permute-start | bytes 786440 | tf_op jit(solution)/shard_map/ppermute | solution.py:180
  99.0 1.7 %collective-permute-start.28 = (bf16[1024,256]{1,0:T(8,128)(2,1)S(1)}, bf16[1024,256]{1,0:T(8,128)(2,1)S(1)}, u32[]{:S(2)}, u32[]{:S(2)}) collective-permute-start(bf16[1024,256]{1,0:T(8,128)(2,1)S(1)} %copy-done.8), channel_id=1, source_target_pairs={{0,4},{4,0},{8,12},{12,8},{1,5},{5,1},{9,13},{13,9},{2,6},{6,2},{1... | collective-permute-start | bytes 1572872 | tf_op jit(solution)/shard_map/ppermute | solution.py:180
  100.7 20.9 %collective-permute-done.27.refs_4_ = bf16[1024,256]{1,0:T(8,128)(2,1)S(1)} collective-permute-done((bf16[1024,256]{1,0:T(8,128)(2,1)S(1)}, bf16[1024,256]{1,0:T(8,128)(2,1)S(1)}, u32[]{:S(2)}, u32[]{:S(2)}) %collective-permute-start.27) | collective-permute-done | bytes 524320 | tf_op jit(solution)/shard_map/ppermute | solution.py:180
  122.3 12.6 %collective-permute-done.29.refs_6_ = bf16[1024,256]{1,0:T(8,128)(2,1)S(1)} collective-permute-done((bf16[1024,256]{1,0:T(8,128)(2,1)S(1)}, bf16[1024,256]{1,0:T(8,128)(2,1)S(1)}, u32[]{:S(2)}, u32[]{:S(2)}) %collective-permute-start.29) | collective-permute-done | bytes 524320 | tf_op jit(solution)/shard_map/ppermute | solution.py:180
  135.0 5.6 %shard_map.205 = (bf16[64,2048]{1,0:T(8,128)(2,1)S(1)}, bf16[64,2048]{1,0:T(8,128)(2,1)S(1)}) custom-call(bf16[64,2048]{1,0:T(8,128)(2,1)S(1)} %get-tuple-element.44.refs_0_, bf16[64,2048]{1,0:T(8,128)(2,1)S(1)} %collective-permute-done.26.refs_1_, bf16[2048,512]{1,0:T(8,128)(2,1)S(1)} %copy-done.5, bf16[1024,256]{1,0:T(8,128)(2,1)S(1)} %copy-done.8, ...), custom_call_target="tpu_custom_call" | custom-call | tf_op jit(solution)/shard_map/pallas_call | solution.py:184
  140.7 1.5 %collective-permute-done.30 = bf16[64,2048]{1,0:T(8,128)(2,1)S(1)} collective-permute-done((bf16[64,2048]{1,0:T(8,128)(2,1)S(1)}, bf16[64,2048]{1,0:T(8,128)(2,1)S(1)}, u32[]{:S(2)}, u32[]{:S(2)}) %collective-permute-start.30) | collective-permute-done | bytes 262176 | tf_op jit(solution)/shard_map/ppermute | solution.py:180
  142.3 1.5 %collective-permute-start.31 = (bf16[32,2048]{1,0:T(8,128)(2,1)S(1)}, bf16[32,2048]{1,0:T(8,128)(2,1)S(1)}, u32[]{:S(2)}, u32[]{:S(2)}) collective-permute-start(bf16[32,2048]{1,0:T(8,128)(2,1)S(1)} %get-tuple-element.53), channel_id=1, source_target_pairs={{0,2},{1,3},{2,0},{3,1},{4,6},{5,7},{6,4},{7,5},{8,10},{9,11},{10,... | collective-permute-start | bytes 393224 | tf_op jit(solution)/shard_map/ppermute | solution.py:180
  143.8 4.1 %collective-permute-done.31.other_ref = bf16[32,2048]{1,0:T(8,128)(2,1)S(1)} collective-permute-done((bf16[32,2048]{1,0:T(8,128)(2,1)S(1)}, bf16[32,2048]{1,0:T(8,128)(2,1)S(1)}, u32[]{:S(2)}, u32[]{:S(2)}) %collective-permute-start.31) | collective-permute-done | bytes 131104 | tf_op jit(solution)/shard_map/ppermute | solution.py:180
  (105 shorter events, 19.4 us)
Async XLA Ops:
  1.4 19.5 %collective-permute-start.7 = (bf16[64,2048]{1,0:T(8,128)(2,1)S(1)}, bf16[64,2048]{1,0:T(8,128)(2,1)S(1)}, u32[]{:S(2)}, u32[]{:S(2)}) collective-permute-start(bf16[64,2048]{1,0:T(8,128)(2,1)S(1)} %get-tuple-element.52.refs_0_), channel_id=1, source_target_pairs={{0,2},{1,3},{2,0},{3,1},{4,6},{5,7},{6,4},{7,5},{8,10},{9,11},{10,... | collective-permute-start | bytes 786440 | tf_op jit(solution)/shard_map/ppermute | solution.py:180
  4.5 16.5 %collective-permute-start.6 = (bf16[64,2048]{1,0:T(8,128)(2,1)S(1)}, bf16[64,2048]{1,0:T(8,128)(2,1)S(1)}, u32[]{:S(2)}, u32[]{:S(2)}) collective-permute-start(bf16[64,2048]{1,0:T(8,128)(2,1)S(1)} %get-tuple-element.52.refs_0_), channel_id=1, source_target_pairs={{0,1},{1,0},{2,3},{3,2},{4,5},{5,4},{6,7},{7,6},{8,9},{9,8},{10,11... | collective-permute-start | bytes 786440 | tf_op jit(solution)/shard_map/ppermute | solution.py:180
  4.5 16.9 %collective-permute-start.10 = (bf16[64,2048]{1,0:T(8,128)(2,1)S(1)}, bf16[64,2048]{1,0:T(8,128)(2,1)S(1)}, u32[]{:S(2)}, u32[]{:S(2)}) collective-permute-start(bf16[64,2048]{1,0:T(8,128)(2,1)S(1)} %get-tuple-element.49.refs_0_), channel_id=1, source_target_pairs={{0,2},{1,3},{2,0},{3,1},{4,6},{5,7},{6,4},{7,5},{8,10},{9,11},{10,... | collective-permute-start | bytes 786440 | tf_op jit(solution)/shard_map/ppermute | solution.py:180
  4.6 17.0 %collective-permute-start.9 = (bf16[64,2048]{1,0:T(8,128)(2,1)S(1)}, bf16[64,2048]{1,0:T(8,128)(2,1)S(1)}, u32[]{:S(2)}, u32[]{:S(2)}) collective-permute-start(bf16[64,2048]{1,0:T(8,128)(2,1)S(1)} %get-tuple-element.49.refs_0_), channel_id=1, source_target_pairs={{0,1},{1,0},{2,3},{3,2},{4,5},{5,4},{6,7},{7,6},{8,9},{9,8},{10,11... | collective-permute-start | bytes 786440 | tf_op jit(solution)/shard_map/ppermute | solution.py:180
  5.0 14.2 %collective-permute-start.12 = (bf16[32,2048]{1,0:T(8,128)(2,1)}, bf16[32,2048]{1,0:T(8,128)(2,1)S(1)}, u32[]{:S(2)}, u32[]{:S(2)}) collective-permute-start(bf16[32,2048]{1,0:T(8,128)(2,1)} %param.20), channel_id=1, source_target_pairs={{0,2},{1,3},{2,0},{3,1},{4,6},{5,7},{6,4},{7,5},{8,10},{9,11},{10,... | collective-permute-start | bytes 393224 | tf_op jit(solution)/shard_map/ppermute | solution.py:180
  19.2 9.2 %collective-permute-start.4 = (bf16[64,2048]{1,0:T(8,128)(2,1)S(1)}, bf16[64,2048]{1,0:T(8,128)(2,1)S(1)}, u32[]{:S(2)}, u32[]{:S(2)}) collective-permute-start(bf16[64,2048]{1,0:T(8,128)(2,1)S(1)} %get-tuple-element.50.refs_0_), channel_id=1, source_target_pairs={{0,2},{1,3},{2,0},{3,1},{4,6},{5,7},{6,4},{7,5},{8,10},{9,11},{10,... | collective-permute-start | bytes 786440 | tf_op jit(solution)/shard_map/ppermute | solution.py:180
  20.9 7.4 %collective-permute-start.3 = (bf16[64,2048]{1,0:T(8,128)(2,1)S(1)}, bf16[64,2048]{1,0:T(8,128)(2,1)S(1)}, u32[]{:S(2)}, u32[]{:S(2)}) collective-permute-start(bf16[64,2048]{1,0:T(8,128)(2,1)S(1)} %get-tuple-element.50.refs_0_), channel_id=1, source_target_pairs={{0,1},{1,0},{2,3},{3,2},{4,5},{5,4},{6,7},{7,6},{8,9},{9,8},{10,11... | collective-permute-start | bytes 786440 | tf_op jit(solution)/shard_map/ppermute | solution.py:180
  21.0 11.3 %collective-permute-start.1 = (bf16[64,2048]{1,0:T(8,128)(2,1)S(1)}, bf16[64,2048]{1,0:T(8,128)(2,1)S(1)}, u32[]{:S(2)}, u32[]{:S(2)}) collective-permute-start(bf16[64,2048]{1,0:T(8,128)(2,1)S(1)} %get-tuple-element.51.refs_0_), channel_id=1, source_target_pairs={{0,2},{1,3},{2,0},{3,1},{4,6},{5,7},{6,4},{7,5},{8,10},{9,11},{10,... | collective-permute-start | bytes 786440 | tf_op jit(solution)/shard_map/ppermute | solution.py:180
  21.3 11.0 %collective-permute-start.13 = (bf16[64,2048]{1,0:T(8,128)(2,1)S(1)}, bf16[64,2048]{1,0:T(8,128)(2,1)S(1)}, u32[]{:S(2)}, u32[]{:S(2)}) collective-permute-start(bf16[64,2048]{1,0:T(8,128)(2,1)S(1)} %constant_dynamic-update-slice_fusion.top_ref.stream_ref), channel_id=1, source_target_pairs={{0,1},{1,0},{2,3},{3,2},{4,5},{5,4},{6,7},{7,6},{8,9},{9,8},{10,11... | collective-permute-start | bytes 786440 | tf_op jit(solution)/shard_map/ppermute | solution.py:180
  21.6 12.8 %collective-permute-start.8 = (bf16[64,2048]{1,0:T(8,128)(2,1)S(1)}, bf16[64,2048]{1,0:T(8,128)(2,1)S(1)}, u32[]{:S(2)}, u32[]{:S(2)}) collective-permute-start(bf16[64,2048]{1,0:T(8,128)(2,1)S(1)} %collective-permute-done.7.refs_2_), channel_id=1, source_target_pairs={{0,1},{1,0},{2,3},{3,2},{4,5},{5,4},{6,7},{7,6},{8,9},{9,8},{10,11... | collective-permute-start | bytes 786440 | tf_op jit(solution)/shard_map/ppermute | solution.py:180
  28.4 9.7 %collective-permute-start.11 = (bf16[64,2048]{1,0:T(8,128)(2,1)S(1)}, bf16[64,2048]{1,0:T(8,128)(2,1)S(1)}, u32[]{:S(2)}, u32[]{:S(2)}) collective-permute-start(bf16[64,2048]{1,0:T(8,128)(2,1)S(1)} %collective-permute-done.10.refs_2_), channel_id=1, source_target_pairs={{0,1},{1,0},{2,3},{3,2},{4,5},{5,4},{6,7},{7,6},{8,9},{9,8},{10,11... | collective-permute-start | bytes 786440 | tf_op jit(solution)/shard_map/ppermute | solution.py:180
  28.4 9.7 %collective-permute-start.5 = (bf16[64,2048]{1,0:T(8,128)(2,1)S(1)}, bf16[64,2048]{1,0:T(8,128)(2,1)S(1)}, u32[]{:S(2)}, u32[]{:S(2)}) collective-permute-start(bf16[64,2048]{1,0:T(8,128)(2,1)S(1)} %collective-permute-done.4.refs_2_), channel_id=1, source_target_pairs={{0,1},{1,0},{2,3},{3,2},{4,5},{5,4},{6,7},{7,6},{8,9},{9,8},{10,11... | collective-permute-start | bytes 786440 | tf_op jit(solution)/shard_map/ppermute | solution.py:180
  32.3 8.9 %collective-permute-start = (bf16[64,2048]{1,0:T(8,128)(2,1)S(1)}, bf16[64,2048]{1,0:T(8,128)(2,1)S(1)}, u32[]{:S(2)}, u32[]{:S(2)}) collective-permute-start(bf16[64,2048]{1,0:T(8,128)(2,1)S(1)} %get-tuple-element.51.refs_0_), channel_id=1, source_target_pairs={{0,1},{1,0},{2,3},{3,2},{4,5},{5,4},{6,7},{7,6},{8,9},{9,8},{10,11... | collective-permute-start | bytes 786440 | tf_op jit(solution)/shard_map/ppermute | solution.py:180
  32.3 8.9 %collective-permute-start.2 = (bf16[64,2048]{1,0:T(8,128)(2,1)S(1)}, bf16[64,2048]{1,0:T(8,128)(2,1)S(1)}, u32[]{:S(2)}, u32[]{:S(2)}) collective-permute-start(bf16[64,2048]{1,0:T(8,128)(2,1)S(1)} %collective-permute-done.1.refs_2_), channel_id=1, source_target_pairs={{0,1},{1,0},{2,3},{3,2},{4,5},{5,4},{6,7},{7,6},{8,9},{9,8},{10,11... | collective-permute-start | bytes 786440 | tf_op jit(solution)/shard_map/ppermute | solution.py:180
  34.4 8.3 %collective-permute-start.18 = (bf16[128,512]{1,0:T(8,128)(2,1)S(1)}, bf16[128,512]{1,0:T(8,128)(2,1)S(1)}, u32[]{:S(2)}, u32[]{:S(2)}) collective-permute-start(bf16[128,512]{1,0:T(8,128)(2,1)S(1)} %shard_map.195.query_ref), channel_id=1, source_target_pairs={{0,12},{4,8},{8,4},{12,0},{1,13},{5,9},{9,5},{13,1},{2,14},{6,10},... | collective-permute-start | bytes 393224 | tf_op jit(solution)/shard_map/ppermute | solution.py:180
  38.1 15.3 %collective-permute-start.16 = (bf16[128,512]{1,0:T(8,128)(2,1)S(1)}, bf16[128,512]{1,0:T(8,128)(2,1)S(1)}, u32[]{:S(2)}, u32[]{:S(2)}) collective-permute-start(bf16[128,512]{1,0:T(8,128)(2,1)S(1)} %shard_map.195.query_ref), channel_id=1, source_target_pairs={{0,8},{4,12},{8,0},{12,4},{1,9},{5,13},{9,1},{13,5},{2,10},{6,14},... | collective-permute-start | bytes 393224 | tf_op jit(solution)/shard_map/ppermute | solution.py:180
  38.1 17.0 %collective-permute-start.14 = (bf16[128,512]{1,0:T(8,128)(2,1)S(1)}, bf16[128,512]{1,0:T(8,128)(2,1)S(1)}, u32[]{:S(2)}, u32[]{:S(2)}) collective-permute-start(bf16[128,512]{1,0:T(8,128)(2,1)S(1)} %shard_map.195.query_ref), channel_id=1, source_target_pairs={{0,4},{4,0},{8,12},{12,8},{1,5},{5,1},{9,13},{13,9},{2,6},{6,2},{1... | collective-permute-start | bytes 393224 | tf_op jit(solution)/shard_map/ppermute | solution.py:180
  44.3 16.9 %collective-permute-start.19 = (bf16[144,512]{1,0:T(8,128)(2,1)S(1)}, bf16[144,512]{1,0:T(8,128)(2,1)S(1)}, u32[]{:S(2)}, u32[]{:S(2)}) collective-permute-start(bf16[144,512]{1,0:T(8,128)(2,1)S(1)} %shard_map.199), channel_id=1, source_target_pairs={{0,12},{4,8},{8,4},{12,0},{1,13},{5,9},{9,5},{13,1},{2,14},{6,10},... | collective-permute-start | bytes 442376 | tf_op jit(solution)/shard_map/ppermute | solution.py:180
  55.0 7.3 %collective-permute-start.17 = (bf16[144,512]{1,0:T(8,128)(2,1)S(1)}, bf16[144,512]{1,0:T(8,128)(2,1)S(1)}, u32[]{:S(2)}, u32[]{:S(2)}) collective-permute-start(bf16[144,512]{1,0:T(8,128)(2,1)S(1)} %shard_map.198), channel_id=1, source_target_pairs={{0,8},{4,12},{8,0},{12,4},{1,9},{5,13},{9,1},{13,5},{2,10},{6,14},... | collective-permute-start | bytes 442376 | tf_op jit(solution)/shard_map/ppermute | solution.py:180
  56.6 6.9 %collective-permute-start.15 = (bf16[144,512]{1,0:T(8,128)(2,1)S(1)}, bf16[144,512]{1,0:T(8,128)(2,1)S(1)}, u32[]{:S(2)}, u32[]{:S(2)}) collective-permute-start(bf16[144,512]{1,0:T(8,128)(2,1)S(1)} %shard_map.197), channel_id=1, source_target_pairs={{0,4},{4,0},{8,12},{12,8},{1,5},{5,1},{9,13},{13,9},{2,6},{6,2},{1... | collective-permute-start | bytes 442376 | tf_op jit(solution)/shard_map/ppermute | solution.py:180
  64.8 1.6 %collective-permute-start.20 = (bf16[64,2048]{1,0:T(8,128)(2,1)S(1)}, bf16[64,2048]{1,0:T(8,128)(2,1)S(1)}, u32[]{:S(2)}, u32[]{:S(2)}) collective-permute-start(bf16[64,2048]{1,0:T(8,128)(2,1)S(1)} %get-tuple-element.36), channel_id=1, source_target_pairs={{0,1},{1,0},{2,3},{3,2},{4,5},{5,4},{6,7},{7,6},{8,9},{9,8},{10,11... | collective-permute-start | bytes 786440 | tf_op jit(solution)/shard_map/ppermute | solution.py:180
  66.4 8.6 %collective-permute-start.21 = (bf16[64,2048]{1,0:T(8,128)(2,1)S(1)}, bf16[64,2048]{1,0:T(8,128)(2,1)S(1)}, u32[]{:S(2)}, u32[]{:S(2)}) collective-permute-start(bf16[64,2048]{1,0:T(8,128)(2,1)S(1)} %add_convert_fusion.2.own_ref), channel_id=1, source_target_pairs={{0,2},{1,3},{2,0},{3,1},{4,6},{5,7},{6,4},{7,5},{8,10},{9,11},{10,... | collective-permute-start | bytes 786440 | tf_op jit(solution)/shard_map/ppermute | solution.py:180
  76.3 7.8 %collective-permute-start.22 = (bf16[64,2048]{1,0:T(8,128)(2,1)S(1)}, bf16[64,2048]{1,0:T(8,128)(2,1)}, u32[]{:S(2)}, u32[]{:S(2)}) collective-permute-start(bf16[64,2048]{1,0:T(8,128)(2,1)S(1)} %get-tuple-element.38.own_ref), channel_id=1, source_target_pairs={{0,1},{1,0},{2,3},{3,2},{4,5},{5,4},{6,7},{7,6},{8,9},{9,8},{10,11... | collective-permute-start | bytes 786440 | tf_op jit(solution)/shard_map/ppermute | solution.py:180
  88.2 5.0 %collective-permute-start.23 = (bf16[16,704]{1,0:T(8,128)(2,1)S(1)}, bf16[16,704]{1,0:T(8,128)(2,1)S(1)}, u32[]{:S(2)}, u32[]{:S(2)}) collective-permute-start(bf16[16,704]{1,0:T(8,128)(2,1)S(1)} %pad_maximum_fusion), channel_id=1, source_target_pairs={{0,4},{4,8},{8,12},{1,5},{5,9},{9,13},{2,6},{6,10},{10,14},{3,7},{... | collective-permute-start | bytes 67592 | tf_op jit(solution)/shard_map/ppermute | solution.py:26
  95.0 2.4 %collective-permute-start.24 = (bf16[64,2048]{1,0:T(8,128)(2,1)S(1)}, bf16[64,2048]{1,0:T(8,128)(2,1)S(1)}, u32[]{:S(2)}, u32[]{:S(2)}) collective-permute-start(bf16[64,2048]{1,0:T(8,128)(2,1)S(1)} %get-tuple-element.42), channel_id=1, source_target_pairs={{0,1},{1,0},{2,3},{3,2},{4,5},{5,4},{6,7},{7,6},{8,9},{9,8},{10,11... | collective-permute-start | bytes 786440 | tf_op jit(solution)/shard_map/ppermute | solution.py:180
  95.1 26.6 %collective-permute-start.27 = (bf16[1024,256]{1,0:T(8,128)(2,1)S(1)}, bf16[1024,256]{1,0:T(8,128)(2,1)S(1)}, u32[]{:S(2)}, u32[]{:S(2)}) collective-permute-start(bf16[1024,256]{1,0:T(8,128)(2,1)S(1)} %copy-done.8), channel_id=1, source_target_pairs={{0,8},{4,12},{8,0},{12,4},{1,9},{5,13},{9,1},{13,5},{2,10},{6,14},... | collective-permute-start | bytes 1572872 | tf_op jit(solution)/shard_map/ppermute | solution.py:180
  97.4 24.5 %collective-permute-start.25 = (bf16[64,2048]{1,0:T(8,128)(2,1)S(1)}, bf16[64,2048]{1,0:T(8,128)(2,1)S(1)}, u32[]{:S(2)}, u32[]{:S(2)}) collective-permute-start(bf16[64,2048]{1,0:T(8,128)(2,1)S(1)} %add_convert_fusion.1.own_ref), channel_id=1, source_target_pairs={{0,2},{1,3},{2,0},{3,1},{4,6},{5,7},{6,4},{7,5},{8,10},{9,11},{10,... | collective-permute-start | bytes 786440 | tf_op jit(solution)/shard_map/ppermute | solution.py:180
  99.0 23.3 %collective-permute-start.28 = (bf16[1024,256]{1,0:T(8,128)(2,1)S(1)}, bf16[1024,256]{1,0:T(8,128)(2,1)S(1)}, u32[]{:S(2)}, u32[]{:S(2)}) collective-permute-start(bf16[1024,256]{1,0:T(8,128)(2,1)S(1)} %copy-done.8), channel_id=1, source_target_pairs={{0,4},{4,0},{8,12},{12,8},{1,5},{5,1},{9,13},{13,9},{2,6},{6,2},{1... | collective-permute-start | bytes 1572872 | tf_op jit(solution)/shard_map/ppermute | solution.py:180
  121.6 13.3 %collective-permute-start.29 = (bf16[1024,256]{1,0:T(8,128)(2,1)S(1)}, bf16[1024,256]{1,0:T(8,128)(2,1)S(1)}, u32[]{:S(2)}, u32[]{:S(2)}) collective-permute-start(bf16[1024,256]{1,0:T(8,128)(2,1)S(1)} %collective-permute-done.27.refs_4_), channel_id=1, source_target_pairs={{0,4},{4,0},{8,12},{12,8},{1,5},{5,1},{9,13},{13,9},{2,6},{6,2},{1... | collective-permute-start | bytes 1572872 | tf_op jit(solution)/shard_map/ppermute | solution.py:180
  122.2 12.7 %collective-permute-start.26 = (bf16[64,2048]{1,0:T(8,128)(2,1)S(1)}, bf16[64,2048]{1,0:T(8,128)(2,1)S(1)}, u32[]{:S(2)}, u32[]{:S(2)}) collective-permute-start(bf16[64,2048]{1,0:T(8,128)(2,1)S(1)} %get-tuple-element.44.refs_0_), channel_id=1, source_target_pairs={{0,1},{1,0},{2,3},{3,2},{4,5},{5,4},{6,7},{7,6},{8,9},{9,8},{10,11... | collective-permute-start | bytes 786440 | tf_op jit(solution)/shard_map/ppermute | solution.py:180
  140.6 1.6 %collective-permute-start.30 = (bf16[64,2048]{1,0:T(8,128)(2,1)S(1)}, bf16[64,2048]{1,0:T(8,128)(2,1)S(1)}, u32[]{:S(2)}, u32[]{:S(2)}) collective-permute-start(bf16[64,2048]{1,0:T(8,128)(2,1)S(1)} %get-tuple-element.47), channel_id=1, source_target_pairs={{0,1},{1,0},{2,3},{3,2},{4,5},{5,4},{6,7},{7,6},{8,9},{9,8},{10,11... | collective-permute-start | bytes 786440 | tf_op jit(solution)/shard_map/ppermute | solution.py:180
  142.3 5.6 %collective-permute-start.31 = (bf16[32,2048]{1,0:T(8,128)(2,1)S(1)}, bf16[32,2048]{1,0:T(8,128)(2,1)S(1)}, u32[]{:S(2)}, u32[]{:S(2)}) collective-permute-start(bf16[32,2048]{1,0:T(8,128)(2,1)S(1)} %get-tuple-element.53), channel_id=1, source_target_pairs={{0,2},{1,3},{2,0},{3,1},{4,6},{5,7},{6,4},{7,5},{8,10},{9,11},{10,... | collective-permute-start | bytes 393224 | tf_op jit(solution)/shard_map/ppermute | solution.py:180
  (21 other events, 442.3 us)

commit v2 on v0

--- a/solution.py
+++ b/solution.py
@@ -1,7 +1,12 @@
+import functools
+
 import jax
 import jax.numpy as jnp
 from jax import lax
+from jax.experimental import pallas as pl
+from jax.experimental.pallas import tpu as pltpu
 from jax.sharding import PartitionSpec as P
+
 
 HEAD = 128
 
@@ -100,7 +105,7 @@
     row_count = queries.shape[0]
     head_count = queries.shape[1] // HEAD
     query_heads = queries.reshape(row_count, head_count, HEAD)
-    best_score, weight_sum, weighted = absorber(
+    _, weight_sum, weighted = absorber(
         query_heads,
         empty_running(row_count, head_count),
         (
@@ -171,6 +176,406 @@
     return attention_layer(after_ffn, pre_second, query_second, 1, out_second, post_second)
 
 
+def swapped_mask(block, axis, mask):
+    count = lax.axis_size(axis)
+    return lax.ppermute(block, axis, [(index, index ^ mask) for index in range(count)])
+
+
+def launch(body, outs, *operands, scratch=(), limit=24):
+    return pl.pallas_call(
+        body,
+        out_shape=outs,
+        scratch_shapes=list(scratch),
+        compiler_params=pltpu.CompilerParams(vmem_limit_bytes=limit << 20),
+    )(*operands)
+
+
+def dot32(left, right):
+    return jnp.dot(left, right, preferred_element_type=jnp.float32)
+
+
+def dot_nt(left, right):
+    return lax.dot_general(
+        left, right, (((1,), (1,)), ((), ())), preferred_element_type=jnp.float32
+    )
+
+
+LOCAL_ORDER = (0, 2, 1, 3)
+RIM_ROWS = 8
+
+
+def last_quarter():
+    mask = lax.axis_index("tp") ^ 3
+    return (mask >> 1) + (mask & 1) * 2
+
+
+def tail_rows(ref, quarter):
+    start = pl.multiple_of((last_quarter() + 1) * quarter - 2 * RIM_ROWS, 2 * RIM_ROWS)
+    return ref[pl.ds(start, 2 * RIM_ROWS)][RIM_ROWS:]
+
+
+def query_body(own_ref, other_ref, gain_ref, weight_ref, out_ref, tail_ref, rows_ref):
+    half = own_ref.shape[0]
+    for index, ref in enumerate((own_ref, other_ref)):
+        here = slice(index * half, (index + 1) * half)
+        rows_ref[here] = ref[...]
+        hidden = normed(ref[...], gain_ref[...]).astype(jnp.bfloat16)
+        out_ref[here] = dot32(hidden, weight_ref[...]).astype(jnp.bfloat16)
+    tail_ref[...] = tail_rows(rows_ref, half // 2)
+
+
+def keyval_body(cut, here_ref, beside_ref, *refs):
+    *row_refs, gain_ref, weight_ref, rows_out, keyval_out = refs
+    start = 0
+    for rows in [ref[cut] for ref in (here_ref, beside_ref)] + [ref[...] for ref in row_refs]:
+        stop = start + rows.shape[0]
+        rows_out[start:stop] = normed(rows, gain_ref[...]).astype(jnp.bfloat16)
+        start = stop
+    keyval_out[...] = dot32(rows_out[...], weight_ref[...]).astype(jnp.bfloat16)
+
+
+def project_body(*refs):
+    *row_refs, weight_ref, out_ref = refs
+    start = 0
+    for ref in row_refs:
+        stop = start + ref.shape[0]
+        out_ref[start:stop] = dot32(ref[...], weight_ref[...]).astype(jnp.bfloat16)
+        start = stop
+
+
+EXPONENT_SCALE = HEAD ** (-0.5) * 1.4426950408889634
+
+
+def head_partial(query, keyval_refs):
+    best = weighted = None
+    for ref in keyval_refs:
+        scores = dot_nt(query, ref[:, :HEAD]) * EXPONENT_SCALE
+        newest = jnp.max(scores, axis=1, keepdims=True)
+        if best is not None:
+            newest = jnp.maximum(best, newest)
+        weights = jnp.exp2(scores - newest).astype(jnp.bfloat16)
+        ones = jnp.ones((ref.shape[0], HEAD), jnp.bfloat16)
+        added = dot32(weights, jnp.concatenate([ref[:, HEAD:], ones], axis=1))
+        weighted = added if best is None else weighted * jnp.exp2(best - newest) + added
+        best = newest
+    return best, weighted[:, HEAD:], weighted[:, :HEAD]
+
+
+STAT_ROWS = 8
+STAT_LANES = 32
+
+
+def partial_body(mask, blocks, *refs):
+    query_refs, keyval_refs, out_ref = refs[:blocks], refs[blocks:-1], refs[-1]
+    rows, width = query_refs[0].shape
+    block = lax.axis_index("sp")
+    before = ((block ^ mask) - 1) ^ block
+    rim = jnp.zeros((RIM_ROWS, width), jnp.bfloat16)
+    for index, ref in enumerate(query_refs):
+        rim = jnp.where(before == index, tail_rows(ref, rows // 4), rim)
+    lane = lax.broadcasted_iota(jnp.int32, (rows + RIM_ROWS, HEAD), 1)
+    levels = jnp.zeros((rows + RIM_ROWS, HEAD), jnp.float32)
+    for head in range(width // HEAD):
+        columns = slice(head * HEAD, (head + 1) * HEAD)
+        query = jnp.concatenate([query_refs[mask][:, columns], rim[:, columns]], axis=0)
+        best, weight_sum, weighted = head_partial(query, keyval_refs)
+        out_ref[: rows + RIM_ROWS, columns] = (weighted / weight_sum).astype(jnp.bfloat16)
+        levels = jnp.where(lane == head, best + jnp.log2(weight_sum), levels)
+    left, rim_left = levels[:rows].T[:STAT_ROWS], levels[rows:, :STAT_LANES]
+    for piece in range(3):
+        for part, place, size in ((left, piece * rows, rows), (rim_left, 3 * rows + piece * STAT_LANES, STAT_LANES)):
+            out_ref[rows + RIM_ROWS :, place : place + size] = part.astype(jnp.bfloat16)
+        left = left - left.astype(jnp.bfloat16).astype(jnp.float32)
+        rim_left = rim_left - rim_left.astype(jnp.bfloat16).astype(jnp.float32)
+
+
+def shares_of(levels):
+    best = functools.reduce(jnp.maximum, levels)
+    shares = [jnp.exp2(level - best) for level in levels]
+    total = functools.reduce(jnp.add, shares)
+    return [share / total for share in shares]
+
+
+def joined_heads(partial_refs, heads_ref):
+    width = heads_ref.shape[1]
+    rows = heads_ref.shape[0] - RIM_ROWS
+
+    def levels(start, size):
+        return [
+            sum(
+                ref[rows + RIM_ROWS :, start + piece * size : start + (piece + 1) * size].astype(jnp.float32)
+                for piece in range(3)
+            )
+            for ref in partial_refs
+        ]
+
+    filler = jnp.zeros((HEAD - STAT_ROWS, rows), jnp.float32)
+    columns = [
+        jnp.concatenate([share, filler], axis=0).T for share in shares_of(levels(0, rows))
+    ]
+    for cut, parts in (
+        (slice(0, rows), columns),
+        (slice(rows, rows + RIM_ROWS), shares_of(levels(3 * rows, STAT_LANES))),
+    ):
+        for head in range(width // HEAD):
+            lanes = slice(head * HEAD, (head + 1) * HEAD)
+            heads_ref[cut, lanes] = sum(
+                ref[cut, lanes].astype(jnp.float32) * part[:, head : head + 1]
+                for ref, part in zip(partial_refs, parts)
+            ).astype(jnp.bfloat16)
+
+
+def join_send_body(*refs):
+    *partial_refs, weight_ref, send_ref, heads_out, heads_ref = refs
+    joined_heads(partial_refs, heads_ref)
+    half = (heads_ref.shape[0] - RIM_ROWS) // 2
+    send_ref[...] = dot32(heads_ref[half:], weight_ref[...]).astype(jnp.bfloat16)
+    heads_out[:half] = heads_ref[:half]
+    heads_out[half:] = heads_ref[2 * half :]
+
+
+def residual_body(own_ref, other_ref, *refs):
+    stream_ref, post_ref, pre_ref, stream_out, hidden_out = refs
+    half = stream_out.shape[0]
+    quarter = half // 2
+    for index in range(2):
+        here = slice(index * quarter, (index + 1) * quarter)
+        there = slice((1 - index) * quarter, (2 - index) * quarter)
+        mixed = own_ref[here].astype(jnp.float32) + other_ref[there].astype(jnp.float32)
+        stream = stream_ref[here].astype(jnp.float32) + normed(mixed, post_ref[...])
+        stream_out[here] = stream
+        hidden_out[here] = normed(stream, pre_ref[...]).astype(jnp.bfloat16)
+
+
+def residual_rim_body(own_ref, other_ref, stream_ref, rim_ref, post_ref, pre_ref, stream_out, hidden_out, rim_out):
+    residual_body(own_ref, other_ref, stream_ref, post_ref, pre_ref, stream_out, hidden_out)
+    half = stream_out.shape[0]
+    mixed = own_ref[half:].astype(jnp.float32) + other_ref[half:].astype(jnp.float32)
+    stream = rim_ref[...].astype(jnp.float32) + normed(mixed, post_ref[...])
+    rim = normed(stream, pre_ref[...])
+    rim_out[...] = jnp.where(lax.axis_index("sp") == 0, 0.0, rim).astype(jnp.bfloat16)
+
+
+def last_body(own_ref, other_ref, stream_ref, post_ref, out_ref):
+    mixed = own_ref[...].astype(jnp.float32) + other_ref[...].astype(jnp.float32)
+    out_ref[...] = stream_ref[...] + normed(mixed, post_ref[...])
+
+
+def mixed_taps(ups, taps_ref):
+    rows = ups.shape[0] - RIM_ROWS
+    return sum(
+        taps_ref[tap : tap + 1] * ups[RIM_ROWS - 2 + tap : RIM_ROWS - 2 + tap + rows].astype(jnp.float32)
+        for tap in range(3)
+    )
+
+
+def mixer_body(
+    own_ref,
+    other_ref,
+    rim_ref,
+    gate_ref,
+    value_ref,
+    conv_gate,
+    conv_value,
+    down_ref,
+    send_ref,
+    gated_out,
+    ups_gate,
+    ups_value,
+    gated_ref,
+):
+    quarter = own_ref.shape[0] // 2
+    place = lax.axis_index("tp")
+    starts = [pl.multiple_of((place ^ mask) * quarter, quarter) for mask in LOCAL_ORDER]
+    rows = jnp.concatenate([own_ref[...], other_ref[...], rim_ref[...]], axis=0)
+    for weight_ref, ups in ((gate_ref, ups_gate), (value_ref, ups_value)):
+        product = dot_nt(rows, weight_ref[...])
+        ups[:RIM_ROWS] = product[4 * quarter :].astype(jnp.bfloat16).astype(jnp.float32)
+        for index, start in enumerate(starts):
+            ups[pl.ds(start + RIM_ROWS, quarter)] = (
+                product[index * quarter : (index + 1) * quarter].astype(jnp.bfloat16).astype(jnp.float32)
+            )
+    gated_ref[...] = (
+        jax.nn.gelu(mixed_taps(ups_gate[...], conv_gate), approximate=True)
+        * mixed_taps(ups_value[...], conv_value)
+    ).astype(jnp.bfloat16)
+    parts = [gated_ref[pl.ds(start, quarter)] for start in starts]
+    send_ref[...] = dot32(jnp.concatenate(parts[2:], axis=0), down_ref[...]).astype(jnp.bfloat16)
+    gated_out[...] = jnp.concatenate(parts[:2], axis=0)
+
+
+def second_body(*refs):
+    own_ref, other_ref, query_ref, *keyval_refs, weight_ref, send_ref, heads_out, queries_ref, heads_ref = refs
+    half = own_ref.shape[0]
+    queries_ref[:half] = dot32(own_ref[...], query_ref[...]).astype(jnp.bfloat16)
+    queries_ref[half:] = dot32(other_ref[...], query_ref[...]).astype(jnp.bfloat16)
+    for head in range(heads_ref.shape[1] // HEAD):
+        columns = slice(head * HEAD, (head + 1) * HEAD)
+        _, weight_sum, weighted = head_partial(queries_ref[:, columns], keyval_refs)
+        heads_ref[:, columns] = (weighted / weight_sum).astype(jnp.bfloat16)
+    send_ref[...] = dot32(heads_ref[half:], weight_ref[...]).astype(jnp.bfloat16)
+    heads_out[...] = heads_ref[:half]
+
+
+def shape_of(rows, columns, dtype=jnp.bfloat16):
+    return jax.ShapeDtypeStruct((rows, columns), dtype)
+
+
+CHUNKS = 2
+
+
+def per_device_paired(
+    target,
+    source,
+    source_gain,
+    pre_first,
+    query_first,
+    keyval_first,
+    out_first,
+    post_first,
+    ffn_pre,
+    w_gate,
+    w_value,
+    conv_gate,
+    conv_value,
+    w_down,
+    ffn_post,
+    pre_second,
+    query_second,
+    keyval_second,
+    out_second,
+    post_second,
+):
+    quarter, width = target.shape
+    half, rows = 2 * quarter, 4 * quarter
+    head_width, keyval_width, hidden_width = query_first.shape[1], keyval_first.shape[1], w_gate.shape[1]
+    sp_count = lax.axis_size("sp")
+    row = lambda gain: gain.reshape(1, -1)
+    swap = lambda value, axis, mask: swapped_mask(value, axis, mask)
+    wide = shape_of(half, width)
+
+    own_target = jnp.concatenate([target, swap(target, "tp", 2)], axis=0)
+    other_target = swap(own_target, "tp", 1)
+    queries, tail = launch(
+        query_body,
+        (shape_of(rows, head_width), shape_of(RIM_ROWS, width)),
+        own_target,
+        other_target,
+        row(pre_first),
+        query_first,
+        scratch=[pltpu.VMEM((rows, width), jnp.bfloat16)],
+    )
+    rim_target = shifted(tail, "sp", 1)
+    across = swap(queries, "sp", 2)
+    query_blocks = (queries, swap(queries, "sp", 1), across, swap(across, "sp", 1))
+
+    span = source.shape[0] // CHUNKS
+    beside = swap(source, "tp", 1)
+    keyvals_first, keyvals_second = [], []
+    for chunk in range(CHUNKS):
+        cut = slice(chunk * span, (chunk + 1) * span)
+        across = swap(source[cut], "tp", 2)
+        chunk_rows, chunk_keyval = launch(
+            functools.partial(keyval_body, cut),
+            (shape_of(4 * span, width), shape_of(4 * span, keyval_width)),
+            source,
+            beside,
+            across,
+            swap(across, "tp", 1),
+            row(source_gain),
+            keyval_first,
+        )
+        keyvals_first.append(chunk_keyval)
+        here = launch(project_body, shape_of(4 * span, keyval_width), chunk_rows, keyval_second)
+        parts = [here]
+        for bit in reversed(range((sp_count - 1).bit_length())):
+            parts += [swap(part, "sp", 1 << bit) for part in parts]
+        keyvals_second += parts
+
+    packed = shape_of(rows + RIM_ROWS + STAT_ROWS, head_width)
+    partials = [None] * sp_count
+    for mask in range(sp_count):
+        partial = launch(
+            functools.partial(partial_body, mask, sp_count), packed, *query_blocks, *keyvals_first
+        )
+        partials[mask] = swap(partial, "sp", mask) if mask else partial
+
+    def pair_sum(send, kept, weight):
+        received = swap(send, "tp", 1)
+        keep = launch(project_body, shape_of(*send.shape), kept, weight)
+        return (keep.astype(jnp.float32) + received.astype(jnp.float32)).astype(jnp.bfloat16)
+
+    def residual(own, post_gain, pre_gain, *streams):
+        other = swap(own, "tp", 2)
+        rims = tuple(shape_of(*stream.shape) for stream in streams[1:])
+        return launch(
+            residual_rim_body if rims else residual_body,
+            (shape_of(half, width, jnp.float32), wide) + rims,
+            own,
+            other,
+            *streams,
+            row(post_gain),
+            row(pre_gain),
+        )
+
+    send, kept = launch(
+        join_send_body,
+        (shape_of(half + RIM_ROWS, width), shape_of(half + RIM_ROWS, head_width)),
+        *partials,
+        out_first,
+        scratch=[pltpu.VMEM((rows + RIM_ROWS, head_width), jnp.bfloat16)],
+    )
+    own = pair_sum(send, kept, out_first)
+    after_first, hidden, rim = residual(own, post_first, ffn_pre, own_target, rim_target)
+    send, kept = launch(
+        mixer_body,
+        (wide, shape_of(half, hidden_width)),
+        hidden,
+        swap(hidden, "tp", 1),
+        rim,
+        w_gate.T,
+        w_value.T,
+        conv_gate,
+        conv_value,
+        w_down,
+        scratch=[pltpu.VMEM((rows + RIM_ROWS, hidden_width), jnp.float32)] * 2
+        + [pltpu.VMEM((rows, hidden_width), jnp.bfloat16)],
+    )
+    own = pair_sum(send, kept, w_down)
+    after_ffn, hidden = residual(own, ffn_post, pre_second, after_first)
+    send, kept = launch(
+        second_body,
+        (wide, shape_of(half, head_width)),
+        hidden,
+        swap(hidden, "tp", 1),
+        query_second,
+        *keyvals_second,
+        out_second,
+        scratch=[pltpu.VMEM((rows, head_width), jnp.bfloat16)] * 2,
+        limit=32,
+    )
+    own = pair_sum(send, kept, out_second)
+    return launch(
+        last_body,
+        shape_of(quarter, width, jnp.float32),
+        own[:quarter],
+        swap(own[quarter:], "tp", 2),
+        after_ffn[:quarter],
+        row(post_second),
+    )
+
+
+def fits(mesh, target, query_first, keyval_first):
+    blocks, places = mesh.shape["sp"], mesh.shape["tp"]
+    return (
+        places == len(LOCAL_ORDER)
+        and blocks == 4
+        and target.shape[0] == mesh.shape["grp"] * blocks * HEAD
+        and keyval_first.shape[1] == 2 * HEAD * places
+        and 3 * HEAD <= query_first.shape[1] // places <= STAT_ROWS * HEAD
+    )
+
+
 def solution(mesh):
     placed = (
         P(("grp", "sp", "tp"), None),
@@ -194,10 +599,18 @@
         P("tp", None),
         P(),
     )
-    return jax.shard_map(
-        per_device,
+    placed_body = lambda body: jax.shard_map(
+        body,
         mesh=mesh,
         in_specs=placed,
         out_specs=P(("grp", "sp", "tp"), None),
         check_vma=False,
     )
+
+
+    def program(*arrays):
+        if not fits(mesh, arrays[0], arrays[4], arrays[5]):
+            return placed_body(per_device)(*arrays)
+        return placed_body(per_device_paired)(*arrays)
+
+    return program

time: 287 us -> 138 us (0.48)
  waiting for transfers between devices: 188 us -> 84.2 us
  matrix products: 34.1 us -> 0 us
  starting transfers between devices: 7.26 us -> 30 us
  blocking collectives: 20.4 us -> 0 us
  Pallas kernels: 0 us -> 20.2 us
  other arithmetic: 17.4 us -> 0.2 us
  between operations: 13.8 us -> 0.37 us
    all_gather x5 -> x0, waiting for transfers between devices: 119 us -> none  [the longest x2 46.3 us: attend_keys(): lax.all_gather(values_t, 'sp', axis=1, tiled=True)]
    ppermute x0 -> x27, waiting for transfers between devices: none -> 82.8 us  [swapped_mask(): lax.ppermute(block, axis, [(index, index ^ mask) for index in range(count)])]
    reduce_scatter x3 -> x0, waiting for transfers between devices: 63.8 us -> none  [summed_rows(): lax.psum_scatter(jnp.dot(parts, weight, preferred_element_type=jnp.float3...]
    dot_general x12 -> x0, matrix products: 34.1 us -> none  [the longest x2 11 us: absorber(): jnp.einsum('ths,ds->thd', weights.astype(jnp.bfloat16), value_block, pref...]
    ppermute x0 -> x27, starting transfers between devices: none -> 25.4 us  [swapped_mask(): lax.ppermute(block, axis, [(index, index ^ mask) for index in range(count)])]
    all_gather x3 -> x0, blocking collectives: 20.4 us -> none  [project_rows(): shard_rows = lax.all_gather(rows_here, 'tp', axis=0, tiled=True)]
    pallas_call x0 -> x18, Pallas kernels: none -> 20.2 us  [launch(): pl.pallas_call(body, out_shape=outs, scratch_shapes=list(scratch), compil...]
    reduce_sum x9 -> x0, other arithmetic: 10.4 us -> none  [the longest x7 7.38 us: normed(): jnp.mean(widened * widened, axis=-1, keepdims=True) + 1e-06]
  transfers between devices with their start and end apart: 10 -> 28, of which waited for: 9 -> 17; matrix products, arithmetic and copies ran while one was open for 6% -> 0% of each run, Pallas kernels for 0% -> 7%
where the time goes in v2:
time: 138 us
  waiting for transfers between devices  84.2 us (61%)
  starting transfers between devices  30 us (22%)
  Pallas kernels  20.2 us (15%)
  local copies, waits for them, and re-layouts  3.11 us (2%)
    ppermute x27, waiting for transfers between devices, swapped_mask(): lax.ppermute(block, axis, [(index, index ^ mask) for index in range(count)])  82.8 us
    ppermute x27, starting transfers between devices, swapped_mask(): lax.ppermute(block, axis, [(index, index ^ mask) for index in range(count)])  25.4 us
    pallas_call x18, Pallas kernels, launch(): pl.pallas_call(body, out_shape=outs, scratch_shapes=list(scratch), compil...  20.2 us
    ppermute x1, starting transfers between devices, shifted(): lax.ppermute(value, axis, [(source, source + steps) for source in range(l...  4.65 us
  transfers between devices with their start and end apart: 28, of which 17 were waited for; matrix products, arithmetic and copies ran while one was open for 0% of the time, Pallas kernels for 7%

profile of v2, /device:TPU:0, one launch (start us, length us, event | category | flops | bytes accessed | tf_op | source)
XLA Modules:
  0.0 138.0 jit_solution(4005037186201314392)
XLA Ops:
  0.0 1.4 fusion
  1.4 3.0 %collective-permute-start.8 = (bf16[128,2048]{1,0:T(8,128)(2,1)S(1)}, bf16[128,2048]{1,0:T(8,128)(2,1)S(1)}, u32[]{:S(2)}, u32[]{:S(2)}) collective-permute-start(bf16[128,2048]{1,0:T(8,128)(2,1)S(1)} %get-tuple-element.39), channel_id=1, source_target_pairs={{0,2},{1,3},{2,0},{3,1},{4,6},{5,7},{6,4},{7,5},{8,10},{9,11},{10,... | collective-permute-start | bytes 1572872 | tf_op jit(solution)/shard_map/ppermute | solution.py:181
  4.6 1.9 %collective-permute-start = (bf16[32,2048]{1,0:T(8,128)(2,1)S(1)}, bf16[32,2048]{1,0:T(8,128)(2,1)S(1)}, u32[]{:S(2)}, u32[]{:S(2)}) collective-permute-start(bf16[32,2048]{1,0:T(8,128)(2,1)S(1)} %copy-done.19), channel_id=1, source_target_pairs={{0,2},{1,3},{2,0},{3,1},{4,6},{5,7},{6,4},{7,5},{8,10},{9,11},{10,... | collective-permute-start | bytes 393224 | tf_op jit(solution)/shard_map/ppermute | solution.py:181
  6.5 10.7 %collective-permute-done.8.refs_0_ = bf16[128,2048]{1,0:T(8,128)(2,1)S(1)} collective-permute-done((bf16[128,2048]{1,0:T(8,128)(2,1)S(1)}, bf16[128,2048]{1,0:T(8,128)(2,1)S(1)}, u32[]{:S(2)}, u32[]{:S(2)}) %collective-permute-start.8) | collective-permute-done | bytes 524320 | tf_op jit(solution)/shard_map/ppermute | solution.py:181
  17.2 13.2 %collective-permute-done = bf16[32,2048]{1,0:T(8,128)(2,1)S(1)} collective-permute-done((bf16[32,2048]{1,0:T(8,128)(2,1)S(1)}, bf16[32,2048]{1,0:T(8,128)(2,1)S(1)}, u32[]{:S(2)}, u32[]{:S(2)}) %collective-permute-start) | collective-permute-done | bytes 131104 | tf_op jit(solution)/shard_map/ppermute | solution.py:181
  32.0 1.6 %copy-done.8 = bf16[2048,512]{1,0:T(8,128)(2,1)S(1)} copy-done((bf16[2048,512]{1,0:T(8,128)(2,1)S(1)}, bf16[2048,512]{1,0:T(8,128)(2,1)}, u32[]{:S(2)}) %copy-start.8) | copy-done | bytes 2097176
  34.6 2.9 %collective-permute-start.3 = (bf16[128,512]{1,0:T(8,128)(2,1)S(1)}, bf16[128,512]{1,0:T(8,128)(2,1)S(1)}, u32[]{:S(2)}, u32[]{:S(2)}) collective-permute-start(bf16[128,512]{1,0:T(8,128)(2,1)S(1)} %get-tuple-element.22.refs_0_), channel_id=1, source_target_pairs={{0,8},{4,12},{8,0},{12,4},{1,9},{5,13},{9,1},{13,5},{2,10},{6,14},... | collective-permute-start | bytes 393224 | tf_op jit(solution)/shard_map/ppermute | solution.py:181
  37.5 1.6 %collective-permute-start.2 = (bf16[128,512]{1,0:T(8,128)(2,1)S(1)}, bf16[128,512]{1,0:T(8,128)(2,1)S(1)}, u32[]{:S(2)}, u32[]{:S(2)}) collective-permute-start(bf16[128,512]{1,0:T(8,128)(2,1)S(1)} %get-tuple-element.22.refs_0_), channel_id=1, source_target_pairs={{0,4},{4,0},{8,12},{12,8},{1,5},{5,1},{9,13},{13,9},{2,6},{6,2},{1... | collective-permute-start | bytes 393224 | tf_op jit(solution)/shard_map/ppermute | solution.py:181
  39.0 5.1 %collective-permute-done.3.refs_2_ = bf16[128,512]{1,0:T(8,128)(2,1)S(1)} collective-permute-done((bf16[128,512]{1,0:T(8,128)(2,1)S(1)}, bf16[128,512]{1,0:T(8,128)(2,1)S(1)}, u32[]{:S(2)}, u32[]{:S(2)}) %collective-permute-start.3) | collective-permute-done | bytes 131104 | tf_op jit(solution)/shard_map/ppermute | solution.py:181
  44.8 1.2 shard_map.192
  46.0 1.2 shard_map.191
  47.3 1.9 %collective-permute-done.4.refs_3_ = bf16[128,512]{1,0:T(8,128)(2,1)S(1)} collective-permute-done((bf16[128,512]{1,0:T(8,128)(2,1)S(1)}, bf16[128,512]{1,0:T(8,128)(2,1)S(1)}, u32[]{:S(2)}, u32[]{:S(2)}) %collective-permute-start.4) | collective-permute-done | bytes 131104 | tf_op jit(solution)/shard_map/ppermute | solution.py:181
  49.1 1.1 shard_map.194
  52.5 3.4 %collective-permute-start.11 = (bf16[144,512]{1,0:T(8,128)(2,1)S(1)}, bf16[144,512]{1,0:T(8,128)(2,1)S(1)}, u32[]{:S(2)}, u32[]{:S(2)}) collective-permute-start(bf16[144,512]{1,0:T(8,128)(2,1)S(1)} %shard_map.195), channel_id=1, source_target_pairs={{0,8},{4,12},{8,0},{12,4},{1,9},{5,13},{9,1},{13,5},{2,10},{6,14},... | collective-permute-start | bytes 442376 | tf_op jit(solution)/shard_map/ppermute | solution.py:181
  57.0 1.1 shard_map.193.refs_0_
  58.2 8.1 %collective-permute-done.11.refs_2_ = bf16[144,512]{1,0:T(8,128)(2,1)S(1)} collective-permute-done((bf16[144,512]{1,0:T(8,128)(2,1)S(1)}, bf16[144,512]{1,0:T(8,128)(2,1)S(1)}, u32[]{:S(2)}, u32[]{:S(2)}) %collective-permute-start.11) | collective-permute-done | bytes 147488 | tf_op jit(solution)/shard_map/ppermute | solution.py:181
  68.9 1.6 %collective-permute-start.14 = (bf16[72,2048]{1,0:T(8,128)(2,1)S(1)}, bf16[72,2048]{1,0:T(8,128)(2,1)S(1)}, u32[]{:S(2)}, u32[]{:S(2)}) collective-permute-start(bf16[72,2048]{1,0:T(8,128)(2,1)S(1)} %add_convert_fusion.own_ref), channel_id=1, source_target_pairs={{0,2},{1,3},{2,0},{3,1},{4,6},{5,7},{6,4},{7,5},{8,10},{9,11},{10,... | collective-permute-start | bytes 884744 | tf_op jit(solution)/shard_map/ppermute | solution.py:181
  70.4 4.7 %collective-permute-start.15 = (bf16[8,2048]{1,0:T(8,128)(2,1)S(1)}, bf16[8,2048]{1,0:T(8,128)(2,1)S(1)}, u32[]{:S(2)}, u32[]{:S(2)}) collective-permute-start(bf16[8,2048]{1,0:T(8,128)(2,1)S(1)} %get-tuple-element.27), channel_id=1, source_target_pairs={{0,4},{4,8},{8,12},{1,5},{5,9},{9,13},{2,6},{6,10},{10,14},{3,7},{... | collective-permute-start | bytes 98312 | tf_op jit(solution)/shard_map/ppermute | solution.py:27
  75.1 1.4 %collective-permute-done.15.rim_ref = bf16[8,2048]{1,0:T(8,128)(2,1)S(1)} collective-permute-done((bf16[8,2048]{1,0:T(8,128)(2,1)S(1)}, bf16[8,2048]{1,0:T(8,128)(2,1)S(1)}, u32[]{:S(2)}, u32[]{:S(2)}) %collective-permute-start.15) | collective-permute-done | bytes 32800 | tf_op jit(solution)/shard_map/ppermute | solution.py:27
  76.5 1.5 %collective-permute-done.14.other_ref = bf16[72,2048]{1,0:T(8,128)(2,1)S(1)} collective-permute-done((bf16[72,2048]{1,0:T(8,128)(2,1)S(1)}, bf16[72,2048]{1,0:T(8,128)(2,1)S(1)}, u32[]{:S(2)}, u32[]{:S(2)}) %collective-permute-start.14) | collective-permute-done | bytes 294944 | tf_op jit(solution)/shard_map/ppermute | solution.py:181
  78.4 1.5 %collective-permute-done.16.other_ref = bf16[64,2048]{1,0:T(8,128)(2,1)S(1)} collective-permute-done((bf16[64,2048]{1,0:T(8,128)(2,1)S(1)}, bf16[64,2048]{1,0:T(8,128)(2,1)S(1)}, u32[]{:S(2)}, u32[]{:S(2)}) %collective-permute-start.16) | collective-permute-done | bytes 262176 | tf_op jit(solution)/shard_map/ppermute | solution.py:181
  80.0 3.0 %shard_map.200 = (bf16[64,2048]{1,0:T(8,128)(2,1)S(1)}, bf16[64,704]{1,0:T(8,128)(2,1)S(1)}) custom-call(bf16[64,2048]{1,0:T(8,128)(2,1)S(1)} %get-tuple-element.28.own_ref, bf16[64,2048]{1,0:T(8,128)(2,1)S(1)} %collective-permute-done.16.other_ref, bf16[8,2048]{1,0:T(8,128)(2,1)S(1)} %get-tuple-element.29.rim_ref, bf16[704,2048]{1,0:T(8,128)(2,1)S(1)} %bitcast.9, ...), custom_call_target="tpu_custom_call" | custom-call | tf_op jit(solution)/shard_map/pallas_call | solution.py:185
  84.6 3.8 %collective-permute-start.20 = (bf16[512,256]{1,0:T(8,128)(2,1)S(1)}, bf16[512,256]{1,0:T(8,128)(2,1)S(1)}, u32[]{:S(2)}, u32[]{:S(2)}) collective-permute-start(bf16[512,256]{1,0:T(8,128)(2,1)S(1)} %shard_map.203.refs_3_), channel_id=1, source_target_pairs={{0,8},{4,12},{8,0},{12,4},{1,9},{5,13},{9,1},{13,5},{2,10},{6,14},... | collective-permute-start | bytes 786440 | tf_op jit(solution)/shard_map/ppermute | solution.py:181
  89.3 1.6 %collective-permute-start.18 = (bf16[64,2048]{1,0:T(8,128)(2,1)S(1)}, bf16[64,2048]{1,0:T(8,128)(2,1)S(1)}, u32[]{:S(2)}, u32[]{:S(2)}) collective-permute-start(bf16[64,2048]{1,0:T(8,128)(2,1)S(1)} %add_convert_fusion.2.own_ref), channel_id=1, source_target_pairs={{0,2},{1,3},{2,0},{3,1},{4,6},{5,7},{6,4},{7,5},{8,10},{9,11},{10,... | collective-permute-start | bytes 786440 | tf_op jit(solution)/shard_map/ppermute | solution.py:181
  90.8 1.7 %collective-permute-start.21 = (bf16[512,256]{1,0:T(8,128)(2,1)S(1)}, bf16[512,256]{1,0:T(8,128)(2,1)S(1)}, u32[]{:S(2)}, u32[]{:S(2)}) collective-permute-start(bf16[512,256]{1,0:T(8,128)(2,1)S(1)} %shard_map.203.refs_3_), channel_id=1, source_target_pairs={{0,4},{4,0},{8,12},{12,8},{1,5},{5,1},{9,13},{13,9},{2,6},{6,2},{1... | collective-permute-start | bytes 786440 | tf_op jit(solution)/shard_map/ppermute | solution.py:181
  92.9 14.1 %collective-permute-done.20.refs_4_ = bf16[512,256]{1,0:T(8,128)(2,1)S(1)} collective-permute-done((bf16[512,256]{1,0:T(8,128)(2,1)S(1)}, bf16[512,256]{1,0:T(8,128)(2,1)S(1)}, u32[]{:S(2)}, u32[]{:S(2)}) %collective-permute-start.20) | collective-permute-done | bytes 262176 | tf_op jit(solution)/shard_map/ppermute | solution.py:181
  107.0 5.3 %collective-permute-done.23.refs_8_ = bf16[512,256]{1,0:T(8,128)(2,1)S(1)} collective-permute-done((bf16[512,256]{1,0:T(8,128)(2,1)S(1)}, bf16[512,256]{1,0:T(8,128)(2,1)S(1)}, u32[]{:S(2)}, u32[]{:S(2)}) %collective-permute-start.23) | collective-permute-done | bytes 262176 | tf_op jit(solution)/shard_map/ppermute | solution.py:181
  112.7 3.2 %collective-permute-done.24.refs_9_ = bf16[512,256]{1,0:T(8,128)(2,1)S(1)} collective-permute-done((bf16[512,256]{1,0:T(8,128)(2,1)S(1)}, bf16[512,256]{1,0:T(8,128)(2,1)S(1)}, u32[]{:S(2)}, u32[]{:S(2)}) %collective-permute-start.24) | collective-permute-done | bytes 262176 | tf_op jit(solution)/shard_map/ppermute | solution.py:181
  115.9 5.6 %collective-permute-done.22.refs_6_ = bf16[512,256]{1,0:T(8,128)(2,1)S(1)} collective-permute-done((bf16[512,256]{1,0:T(8,128)(2,1)S(1)}, bf16[512,256]{1,0:T(8,128)(2,1)S(1)}, u32[]{:S(2)}, u32[]{:S(2)}) %collective-permute-start.22) | collective-permute-done | bytes 262176 | tf_op jit(solution)/shard_map/ppermute | solution.py:181
  121.5 4.5 %collective-permute-done.25.refs_10_ = bf16[512,256]{1,0:T(8,128)(2,1)S(1)} collective-permute-done((bf16[512,256]{1,0:T(8,128)(2,1)S(1)}, bf16[512,256]{1,0:T(8,128)(2,1)S(1)}, u32[]{:S(2)}, u32[]{:S(2)}) %collective-permute-start.25) | collective-permute-done | bytes 262176 | tf_op jit(solution)/shard_map/ppermute | solution.py:181
  126.0 3.9 %shard_map.205 = (bf16[64,2048]{1,0:T(8,128)(2,1)S(1)}, bf16[64,512]{1,0:T(8,128)(2,1)S(1)}) custom-call(bf16[64,2048]{1,0:T(8,128)(2,1)S(1)} %get-tuple-element.33.refs_0_, bf16[64,2048]{1,0:T(8,128)(2,1)S(1)} %collective-permute-done.19.refs_1_, bf16[2048,512]{1,0:T(8,128)(2,1)S(1)} %copy-done.9, bf16[512,256]{1,0:T(8,128)(2,1)S(1)} %shard_map.203.refs_3_, ...), custom_call_target="tpu_custom_call" | custom-call | tf_op jit(solution)/shard_map/pallas_call | solution.py:185
  132.2 5.0 %collective-permute-done.27.other_ref = bf16[32,2048]{1,0:T(8,128)(2,1)S(1)} collective-permute-done((bf16[32,2048]{1,0:T(8,128)(2,1)S(1)}, bf16[32,2048]{1,0:T(8,128)(2,1)S(1)}, u32[]{:S(2)}, u32[]{:S(2)}) %collective-permute-start.27) | collective-permute-done | bytes 131104 | tf_op jit(solution)/shard_map/ppermute | solution.py:181
  (90 shorter events, 16.1 us)
Async XLA Ops:
  0.0 44.8 %copy-start.10 = (f32[2048]{0:T(1024)S(1)}, f32[2048]{0:T(1024)}, u32[]{:S(2)}) copy-start(f32[2048]{0:T(1024)} %param.22) | copy-start | bytes 24580
  1.4 43.4 %copy-start.5 = (bf16[2048,256]{1,0:T(8,128)(2,1)S(1)}, bf16[2048,256]{1,0:T(8,128)(2,1)}, u32[]{:S(2)}) copy-start(bf16[2048,256]{1,0:T(8,128)(2,1)} %refs_3_.3) | copy-start | bytes 3145732
  1.4 15.8 %collective-permute-start.8 = (bf16[128,2048]{1,0:T(8,128)(2,1)S(1)}, bf16[128,2048]{1,0:T(8,128)(2,1)S(1)}, u32[]{:S(2)}, u32[]{:S(2)}) collective-permute-start(bf16[128,2048]{1,0:T(8,128)(2,1)S(1)} %get-tuple-element.39), channel_id=1, source_target_pairs={{0,2},{1,3},{2,0},{3,1},{4,6},{5,7},{6,4},{7,5},{8,10},{9,11},{10,... | collective-permute-start | bytes 1572872 | tf_op jit(solution)/shard_map/ppermute | solution.py:181
  4.4 40.4 %collective-permute-start.5 = (bf16[256,2048]{1,0:T(8,128)(2,1)S(1)}, bf16[256,2048]{1,0:T(8,128)(2,1)S(1)}, u32[]{:S(2)}, u32[]{:S(2)}) collective-permute-start(bf16[256,2048]{1,0:T(8,128)(2,1)S(1)} %copy-done.1), channel_id=1, source_target_pairs={{0,1},{1,0},{2,3},{3,2},{4,5},{5,4},{6,7},{7,6},{8,9},{9,8},{10,11... | collective-permute-start | bytes 3145736 | tf_op jit(solution)/shard_map/ppermute | solution.py:181
  4.4 26.1 %collective-permute-start.6 = (bf16[128,2048]{1,0:T(8,128)(2,1)S(1)}, bf16[128,2048]{1,0:T(8,128)(2,1)S(1)}, u32[]{:S(2)}, u32[]{:S(2)}) collective-permute-start(bf16[128,2048]{1,0:T(8,128)(2,1)S(1)} %get-tuple-element.40), channel_id=1, source_target_pairs={{0,2},{1,3},{2,0},{3,1},{4,6},{5,7},{6,4},{7,5},{8,10},{9,11},{10,... | collective-permute-start | bytes 1572872 | tf_op jit(solution)/shard_map/ppermute | solution.py:181
  4.6 25.8 %collective-permute-start = (bf16[32,2048]{1,0:T(8,128)(2,1)S(1)}, bf16[32,2048]{1,0:T(8,128)(2,1)S(1)}, u32[]{:S(2)}, u32[]{:S(2)}) collective-permute-start(bf16[32,2048]{1,0:T(8,128)(2,1)S(1)} %copy-done.19), channel_id=1, source_target_pairs={{0,2},{1,3},{2,0},{3,1},{4,6},{5,7},{6,4},{7,5},{8,10},{9,11},{10,... | collective-permute-start | bytes 393224 | tf_op jit(solution)/shard_map/ppermute | solution.py:181
  17.2 27.6 %collective-permute-start.9 = (bf16[128,2048]{1,0:T(8,128)(2,1)S(1)}, bf16[128,2048]{1,0:T(8,128)(2,1)S(1)}, u32[]{:S(2)}, u32[]{:S(2)}) collective-permute-start(bf16[128,2048]{1,0:T(8,128)(2,1)S(1)} %collective-permute-done.8.refs_0_), channel_id=1, source_target_pairs={{0,1},{1,0},{2,3},{3,2},{4,5},{5,4},{6,7},{7,6},{8,9},{9,8},{10,11... | collective-permute-start | bytes 1572872 | tf_op jit(solution)/shard_map/ppermute | solution.py:181
  30.4 1.6 %collective-permute-start.1 = (bf16[64,2048]{1,0:T(8,128)(2,1)S(1)}, bf16[64,2048]{1,0:T(8,128)(2,1)S(1)}, u32[]{:S(2)}, u32[]{:S(2)}) collective-permute-start(bf16[64,2048]{1,0:T(8,128)(2,1)S(1)} %constant_dynamic-update-slice_fusion.own_ref.stream_ref), channel_id=1, source_target_pairs={{0,1},{1,0},{2,3},{3,2},{4,5},{5,4},{6,7},{7,6},{8,9},{9,8},{10,11... | collective-permute-start | bytes 786440 | tf_op jit(solution)/shard_map/ppermute | solution.py:181
  30.5 15.5 %collective-permute-start.7 = (bf16[128,2048]{1,0:T(8,128)(2,1)S(1)}, bf16[128,2048]{1,0:T(8,128)(2,1)S(1)}, u32[]{:S(2)}, u32[]{:S(2)}) collective-permute-start(bf16[128,2048]{1,0:T(8,128)(2,1)S(1)} %collective-permute-done.6.refs_0_), channel_id=1, source_target_pairs={{0,1},{1,0},{2,3},{3,2},{4,5},{5,4},{6,7},{7,6},{8,9},{9,8},{10,11... | collective-permute-start | bytes 1572872 | tf_op jit(solution)/shard_map/ppermute | solution.py:181
  34.6 9.6 %collective-permute-start.3 = (bf16[128,512]{1,0:T(8,128)(2,1)S(1)}, bf16[128,512]{1,0:T(8,128)(2,1)S(1)}, u32[]{:S(2)}, u32[]{:S(2)}) collective-permute-start(bf16[128,512]{1,0:T(8,128)(2,1)S(1)} %get-tuple-element.22.refs_0_), channel_id=1, source_target_pairs={{0,8},{4,12},{8,0},{12,4},{1,9},{5,13},{9,1},{13,5},{2,10},{6,14},... | collective-permute-start | bytes 393224 | tf_op jit(solution)/shard_map/ppermute | solution.py:181
  37.5 9.8 %collective-permute-start.2 = (bf16[128,512]{1,0:T(8,128)(2,1)S(1)}, bf16[128,512]{1,0:T(8,128)(2,1)S(1)}, u32[]{:S(2)}, u32[]{:S(2)}) collective-permute-start(bf16[128,512]{1,0:T(8,128)(2,1)S(1)} %get-tuple-element.22.refs_0_), channel_id=1, source_target_pairs={{0,4},{4,0},{8,12},{12,8},{1,5},{5,1},{9,13},{13,9},{2,6},{6,2},{1... | collective-permute-start | bytes 393224 | tf_op jit(solution)/shard_map/ppermute | solution.py:181
  44.2 5.0 %collective-permute-start.4 = (bf16[128,512]{1,0:T(8,128)(2,1)S(1)}, bf16[128,512]{1,0:T(8,128)(2,1)S(1)}, u32[]{:S(2)}, u32[]{:S(2)}) collective-permute-start(bf16[128,512]{1,0:T(8,128)(2,1)S(1)} %collective-permute-done.3.refs_2_), channel_id=1, source_target_pairs={{0,4},{4,0},{8,12},{12,8},{1,5},{5,1},{9,13},{13,9},{2,6},{6,2},{1... | collective-permute-start | bytes 393224 | tf_op jit(solution)/shard_map/ppermute | solution.py:181
  50.3 7.9 %collective-permute-start.10 = (bf16[144,512]{1,0:T(8,128)(2,1)S(1)}, bf16[144,512]{1,0:T(8,128)(2,1)S(1)}, u32[]{:S(2)}, u32[]{:S(2)}) collective-permute-start(bf16[144,512]{1,0:T(8,128)(2,1)S(1)} %shard_map.194), channel_id=1, source_target_pairs={{0,4},{4,0},{8,12},{12,8},{1,5},{5,1},{9,13},{13,9},{2,6},{6,2},{1... | collective-permute-start | bytes 442376 | tf_op jit(solution)/shard_map/ppermute | solution.py:181
  52.5 13.8 %collective-permute-start.11 = (bf16[144,512]{1,0:T(8,128)(2,1)S(1)}, bf16[144,512]{1,0:T(8,128)(2,1)S(1)}, u32[]{:S(2)}, u32[]{:S(2)}) collective-permute-start(bf16[144,512]{1,0:T(8,128)(2,1)S(1)} %shard_map.195), channel_id=1, source_target_pairs={{0,8},{4,12},{8,0},{12,4},{1,9},{5,13},{9,1},{13,5},{2,10},{6,14},... | collective-permute-start | bytes 442376 | tf_op jit(solution)/shard_map/ppermute | solution.py:181
  57.0 9.2 %collective-permute-start.12 = (bf16[144,512]{1,0:T(8,128)(2,1)S(1)}, bf16[144,512]{1,0:T(8,128)(2,1)S(1)}, u32[]{:S(2)}, u32[]{:S(2)}) collective-permute-start(bf16[144,512]{1,0:T(8,128)(2,1)S(1)} %shard_map.196), channel_id=1, source_target_pairs={{0,12},{4,8},{8,4},{12,0},{1,13},{5,9},{9,5},{13,1},{2,14},{6,10},... | collective-permute-start | bytes 442376 | tf_op jit(solution)/shard_map/ppermute | solution.py:181
  67.2 1.6 %collective-permute-start.13 = (bf16[72,2048]{1,0:T(8,128)(2,1)S(1)}, bf16[72,2048]{1,0:T(8,128)(2,1)S(1)}, u32[]{:S(2)}, u32[]{:S(2)}) collective-permute-start(bf16[72,2048]{1,0:T(8,128)(2,1)S(1)} %get-tuple-element.26), channel_id=1, source_target_pairs={{0,1},{1,0},{2,3},{3,2},{4,5},{5,4},{6,7},{7,6},{8,9},{9,8},{10,11... | collective-permute-start | bytes 884744 | tf_op jit(solution)/shard_map/ppermute | solution.py:181
  68.9 9.1 %collective-permute-start.14 = (bf16[72,2048]{1,0:T(8,128)(2,1)S(1)}, bf16[72,2048]{1,0:T(8,128)(2,1)S(1)}, u32[]{:S(2)}, u32[]{:S(2)}) collective-permute-start(bf16[72,2048]{1,0:T(8,128)(2,1)S(1)} %add_convert_fusion.own_ref), channel_id=1, source_target_pairs={{0,2},{1,3},{2,0},{3,1},{4,6},{5,7},{6,4},{7,5},{8,10},{9,11},{10,... | collective-permute-start | bytes 884744 | tf_op jit(solution)/shard_map/ppermute | solution.py:181
  70.4 6.1 %collective-permute-start.15 = (bf16[8,2048]{1,0:T(8,128)(2,1)S(1)}, bf16[8,2048]{1,0:T(8,128)(2,1)S(1)}, u32[]{:S(2)}, u32[]{:S(2)}) collective-permute-start(bf16[8,2048]{1,0:T(8,128)(2,1)S(1)} %get-tuple-element.27), channel_id=1, source_target_pairs={{0,4},{4,8},{8,12},{1,5},{5,9},{9,13},{2,6},{6,10},{10,14},{3,7},{... | collective-permute-start | bytes 98312 | tf_op jit(solution)/shard_map/ppermute | solution.py:27
  78.4 1.6 %collective-permute-start.16 = (bf16[64,2048]{1,0:T(8,128)(2,1)S(1)}, bf16[64,2048]{1,0:T(8,128)(2,1)S(1)}, u32[]{:S(2)}, u32[]{:S(2)}) collective-permute-start(bf16[64,2048]{1,0:T(8,128)(2,1)S(1)} %get-tuple-element.28.own_ref), channel_id=1, source_target_pairs={{0,1},{1,0},{2,3},{3,2},{4,5},{5,4},{6,7},{7,6},{8,9},{9,8},{10,11... | collective-permute-start | bytes 786440 | tf_op jit(solution)/shard_map/ppermute | solution.py:181
  83.0 6.2 %collective-permute-start.17 = (bf16[64,2048]{1,0:T(8,128)(2,1)S(1)}, bf16[64,2048]{1,0:T(8,128)(2,1)S(1)}, u32[]{:S(2)}, u32[]{:S(2)}) collective-permute-start(bf16[64,2048]{1,0:T(8,128)(2,1)S(1)} %get-tuple-element.31), channel_id=1, source_target_pairs={{0,1},{1,0},{2,3},{3,2},{4,5},{5,4},{6,7},{7,6},{8,9},{9,8},{10,11... | collective-permute-start | bytes 786440 | tf_op jit(solution)/shard_map/ppermute | solution.py:181
  84.6 22.3 %collective-permute-start.20 = (bf16[512,256]{1,0:T(8,128)(2,1)S(1)}, bf16[512,256]{1,0:T(8,128)(2,1)S(1)}, u32[]{:S(2)}, u32[]{:S(2)}) collective-permute-start(bf16[512,256]{1,0:T(8,128)(2,1)S(1)} %shard_map.203.refs_3_), channel_id=1, source_target_pairs={{0,8},{4,12},{8,0},{12,4},{1,9},{5,13},{9,1},{13,5},{2,10},{6,14},... | collective-permute-start | bytes 786440 | tf_op jit(solution)/shard_map/ppermute | solution.py:181
  88.5 23.8 %collective-permute-start.23 = (bf16[512,256]{1,0:T(8,128)(2,1)S(1)}, bf16[512,256]{1,0:T(8,128)(2,1)S(1)}, u32[]{:S(2)}, u32[]{:S(2)}) collective-permute-start(bf16[512,256]{1,0:T(8,128)(2,1)S(1)} %shard_map.204.refs_7_), channel_id=1, source_target_pairs={{0,8},{4,12},{8,0},{12,4},{1,9},{5,13},{9,1},{13,5},{2,10},{6,14},... | collective-permute-start | bytes 786440 | tf_op jit(solution)/shard_map/ppermute | solution.py:181
  88.5 37.4 %copy-start.3 = (bf16[512,2048]{1,0:T(8,128)(2,1)S(1)}, bf16[512,2048]{1,0:T(8,128)(2,1)}, u32[]{:S(2)}) copy-start(bf16[512,2048]{1,0:T(8,128)(2,1)} %refs_1_.9) | copy-start | bytes 6291460
  88.5 37.4 %copy-start.9 = (bf16[2048,512]{1,0:T(8,128)(2,1)S(1)}, bf16[2048,512]{1,0:T(8,128)(2,1)}, u32[]{:S(2)}) copy-start(bf16[2048,512]{1,0:T(8,128)(2,1)} %refs_2_.1) | copy-start | bytes 6291460
  89.3 23.0 %collective-permute-start.18 = (bf16[64,2048]{1,0:T(8,128)(2,1)S(1)}, bf16[64,2048]{1,0:T(8,128)(2,1)S(1)}, u32[]{:S(2)}, u32[]{:S(2)}) collective-permute-start(bf16[64,2048]{1,0:T(8,128)(2,1)S(1)} %add_convert_fusion.2.own_ref), channel_id=1, source_target_pairs={{0,2},{1,3},{2,0},{3,1},{4,6},{5,7},{6,4},{7,5},{8,10},{9,11},{10,... | collective-permute-start | bytes 786440 | tf_op jit(solution)/shard_map/ppermute | solution.py:181
  90.8 21.9 %collective-permute-start.21 = (bf16[512,256]{1,0:T(8,128)(2,1)S(1)}, bf16[512,256]{1,0:T(8,128)(2,1)S(1)}, u32[]{:S(2)}, u32[]{:S(2)}) collective-permute-start(bf16[512,256]{1,0:T(8,128)(2,1)S(1)} %shard_map.203.refs_3_), channel_id=1, source_target_pairs={{0,4},{4,0},{8,12},{12,8},{1,5},{5,1},{9,13},{13,9},{2,6},{6,2},{1... | collective-permute-start | bytes 786440 | tf_op jit(solution)/shard_map/ppermute | solution.py:181
  92.5 23.4 %collective-permute-start.24 = (bf16[512,256]{1,0:T(8,128)(2,1)S(1)}, bf16[512,256]{1,0:T(8,128)(2,1)S(1)}, u32[]{:S(2)}, u32[]{:S(2)}) collective-permute-start(bf16[512,256]{1,0:T(8,128)(2,1)S(1)} %shard_map.204.refs_7_), channel_id=1, source_target_pairs={{0,4},{4,0},{8,12},{12,8},{1,5},{5,1},{9,13},{13,9},{2,6},{6,2},{1... | collective-permute-start | bytes 786440 | tf_op jit(solution)/shard_map/ppermute | solution.py:181
  107.0 14.5 %collective-permute-start.22 = (bf16[512,256]{1,0:T(8,128)(2,1)S(1)}, bf16[512,256]{1,0:T(8,128)(2,1)S(1)}, u32[]{:S(2)}, u32[]{:S(2)}) collective-permute-start(bf16[512,256]{1,0:T(8,128)(2,1)S(1)} %collective-permute-done.20.refs_4_), channel_id=1, source_target_pairs={{0,4},{4,0},{8,12},{12,8},{1,5},{5,1},{9,13},{13,9},{2,6},{6,2},{1... | collective-permute-start | bytes 786440 | tf_op jit(solution)/shard_map/ppermute | solution.py:181
  112.3 13.7 %collective-permute-start.25 = (bf16[512,256]{1,0:T(8,128)(2,1)S(1)}, bf16[512,256]{1,0:T(8,128)(2,1)S(1)}, u32[]{:S(2)}, u32[]{:S(2)}) collective-permute-start(bf16[512,256]{1,0:T(8,128)(2,1)S(1)} %collective-permute-done.23.refs_8_), channel_id=1, source_target_pairs={{0,4},{4,0},{8,12},{12,8},{1,5},{5,1},{9,13},{13,9},{2,6},{6,2},{1... | collective-permute-start | bytes 786440 | tf_op jit(solution)/shard_map/ppermute | solution.py:181
  112.6 13.3 %collective-permute-start.19 = (bf16[64,2048]{1,0:T(8,128)(2,1)S(1)}, bf16[64,2048]{1,0:T(8,128)(2,1)S(1)}, u32[]{:S(2)}, u32[]{:S(2)}) collective-permute-start(bf16[64,2048]{1,0:T(8,128)(2,1)S(1)} %get-tuple-element.33.refs_0_), channel_id=1, source_target_pairs={{0,1},{1,0},{2,3},{3,2},{4,5},{5,4},{6,7},{7,6},{8,9},{9,8},{10,11... | collective-permute-start | bytes 786440 | tf_op jit(solution)/shard_map/ppermute | solution.py:181
  129.9 1.6 %collective-permute-start.26 = (bf16[64,2048]{1,0:T(8,128)(2,1)S(1)}, bf16[64,2048]{1,0:T(8,128)(2,1)S(1)}, u32[]{:S(2)}, u32[]{:S(2)}) collective-permute-start(bf16[64,2048]{1,0:T(8,128)(2,1)S(1)} %get-tuple-element.37), channel_id=1, source_target_pairs={{0,1},{1,0},{2,3},{3,2},{4,5},{5,4},{6,7},{7,6},{8,9},{9,8},{10,11... | collective-permute-start | bytes 786440 | tf_op jit(solution)/shard_map/ppermute | solution.py:181
  131.6 5.6 %collective-permute-start.27 = (bf16[32,2048]{1,0:T(8,128)(2,1)S(1)}, bf16[32,2048]{1,0:T(8,128)(2,1)S(1)}, u32[]{:S(2)}, u32[]{:S(2)}) collective-permute-start(bf16[32,2048]{1,0:T(8,128)(2,1)S(1)} %get-tuple-element.41), channel_id=1, source_target_pairs={{0,2},{1,3},{2,0},{3,1},{4,6},{5,7},{6,4},{7,5},{8,10},{9,11},{10,... | collective-permute-start | bytes 393224 | tf_op jit(solution)/shard_map/ppermute | solution.py:181
  (16 other events, 223.1 us)

commit v3 on v2

--- a/solution.py
+++ b/solution.py
@@ -181,7 +181,29 @@
     return lax.ppermute(block, axis, [(index, index ^ mask) for index in range(count)])
 
 
-def launch(body, outs, *operands, scratch=(), limit=24):
+def fetched(*arrays):
+    count = len(arrays)
+
+    def body(*refs):
+        copies = [
+            pltpu.make_async_copy(ref, out_ref, refs[-1].at[index])
+            for index, (ref, out_ref) in enumerate(zip(refs[:count], refs[count:]))
+        ]
+        for copy in copies:
+            copy.start()
+        for copy in copies:
+            copy.wait()
+
+    return pl.pallas_call(
+        body,
+        out_shape=tuple(jax.ShapeDtypeStruct(array.shape, array.dtype) for array in arrays),
+        in_specs=[pl.BlockSpec(memory_space=pl.ANY)] * count,
+        scratch_shapes=[pltpu.SemaphoreType.DMA((count,))],
+        compiler_params=pltpu.CompilerParams(vmem_limit_bytes=6 << 20),
+    )(*arrays)
+
+
+def launch(body, outs, *operands, scratch=(), limit=10):
     return pl.pallas_call(
         body,
         out_shape=outs,
@@ -194,44 +216,72 @@
     return jnp.dot(left, right, preferred_element_type=jnp.float32)
 
 
+LOCAL_ORDER = (0, 2, 1, 3)
+RIM_ROWS = 8
+
+
+def last_quarter():
+    mask = lax.axis_index("tp") ^ 3
+    return (mask >> 1) + (mask & 1) * 2
+
+
+def tail_rows(ref, quarter):
+    start = pl.multiple_of((last_quarter() + 1) * quarter - 2 * RIM_ROWS, 2 * RIM_ROWS)
+    return ref[pl.ds(start, 2 * RIM_ROWS)][RIM_ROWS:]
+
+
 def dot_nt(left, right):
     return lax.dot_general(
         left, right, (((1,), (1,)), ((), ())), preferred_element_type=jnp.float32
     )
 
 
-LOCAL_ORDER = (0, 2, 1, 3)
-RIM_ROWS = 8
-
-
-def last_quarter():
-    mask = lax.axis_index("tp") ^ 3
-    return (mask >> 1) + (mask & 1) * 2
-
-
-def tail_rows(ref, quarter):
-    start = pl.multiple_of((last_quarter() + 1) * quarter - 2 * RIM_ROWS, 2 * RIM_ROWS)
-    return ref[pl.ds(start, 2 * RIM_ROWS)][RIM_ROWS:]
-
-
-def query_body(own_ref, other_ref, gain_ref, weight_ref, out_ref, tail_ref, rows_ref):
+def query_body(own_ref, other_ref, gain_ref, weight_ref, out_ref, rows_ref):
     half = own_ref.shape[0]
     for index, ref in enumerate((own_ref, other_ref)):
         here = slice(index * half, (index + 1) * half)
-        rows_ref[here] = ref[...]
+        rows_ref[here] = ref[...].astype(jnp.float32)
         hidden = normed(ref[...], gain_ref[...]).astype(jnp.bfloat16)
         out_ref[here] = dot32(hidden, weight_ref[...]).astype(jnp.bfloat16)
-    tail_ref[...] = tail_rows(rows_ref, half // 2)
-
-
-def keyval_body(cut, here_ref, beside_ref, *refs):
-    *row_refs, gain_ref, weight_ref, rows_out, keyval_out = refs
-    start = 0
-    for rows in [ref[cut] for ref in (here_ref, beside_ref)] + [ref[...] for ref in row_refs]:
-        stop = start + rows.shape[0]
-        rows_out[start:stop] = normed(rows, gain_ref[...]).astype(jnp.bfloat16)
-        start = stop
-    keyval_out[...] = dot32(rows_out[...], weight_ref[...]).astype(jnp.bfloat16)
+    width = out_ref.shape[1]
+    tail = tail_rows(rows_ref, half // 2)
+    out_ref[2 * half :] = jnp.concatenate(
+        [
+            tail[RIM_ROWS - 2 + index : RIM_ROWS - 1 + index, start : start + width]
+            for index in range(2)
+            for start in range(0, tail.shape[1], width)
+        ],
+        axis=0,
+    ).astype(jnp.bfloat16)
+
+
+def one_before(mask, block):
+    return ((block ^ mask) - 1) ^ block
+
+
+def chosen_part(parts, wanted):
+    result = jnp.zeros(parts[0].shape, parts[0].dtype)
+    for index, part in enumerate(parts):
+        result = jnp.where(wanted == index, part, result)
+    return result
+
+
+def keyval_body(row_ref, gain_ref, mine_ref, theirs_ref, rows_out, mine_out, theirs_out):
+    rows_out[...] = normed(row_ref[...], gain_ref[...]).astype(jnp.bfloat16)
+    for weight_ref, out_ref in ((theirs_ref, theirs_out), (mine_ref, mine_out)):
+        out_ref[...] = dot32(rows_out[...], weight_ref[...]).astype(jnp.bfloat16)
+
+
+def keyval_later_body(*refs):
+    *row_refs, mine_ref, theirs_ref, keyval_out, theirs_out = refs
+    rows = jnp.concatenate([ref[...] for ref in row_refs], axis=0)
+    for weight_ref, out_ref in ((theirs_ref, theirs_out), (mine_ref, keyval_out)):
+        out_ref[...] = dot32(rows, weight_ref[...]).astype(jnp.bfloat16)
+
+
+def turn_body(*refs):
+    for ref, out_ref in zip(refs[: len(refs) // 2], refs[len(refs) // 2 :]):
+        out_ref[...] = ref[...].T
 
 
 def project_body(*refs):
@@ -246,45 +296,59 @@
 EXPONENT_SCALE = HEAD ** (-0.5) * 1.4426950408889634
 
 
+def grouped(refs, size=4 * HEAD):
+    groups, held = [], size
+    for ref in refs:
+        if held >= size:
+            groups.append([])
+            held = 0
+        groups[-1].append(ref)
+        held += ref.shape[0]
+    return groups
+
+
 def head_partial(query, keyval_refs):
     best = weighted = None
-    for ref in keyval_refs:
-        scores = dot_nt(query, ref[:, :HEAD]) * EXPONENT_SCALE
+    for group in grouped(keyval_refs):
+        keys, values = (
+            jnp.concatenate([ref[:, cut] for ref in group], axis=0)
+            for cut in (slice(None, HEAD), slice(HEAD, None))
+        )
+        scores = dot_nt(query, keys) * EXPONENT_SCALE
         newest = jnp.max(scores, axis=1, keepdims=True)
         if best is not None:
             newest = jnp.maximum(best, newest)
         weights = jnp.exp2(scores - newest).astype(jnp.bfloat16)
-        ones = jnp.ones((ref.shape[0], HEAD), jnp.bfloat16)
-        added = dot32(weights, jnp.concatenate([ref[:, HEAD:], ones], axis=1))
+        added = dot32(weights, jnp.concatenate([values, jnp.ones_like(values)], axis=1))
         weighted = added if best is None else weighted * jnp.exp2(best - newest) + added
         best = newest
     return best, weighted[:, HEAD:], weighted[:, :HEAD]
 
 
-STAT_ROWS = 8
-STAT_LANES = 32
-
-
 def partial_body(mask, blocks, *refs):
     query_refs, keyval_refs, out_ref = refs[:blocks], refs[blocks:-1], refs[-1]
-    rows, width = query_refs[0].shape
-    block = lax.axis_index("sp")
-    before = ((block ^ mask) - 1) ^ block
-    rim = jnp.zeros((RIM_ROWS, width), jnp.bfloat16)
-    for index, ref in enumerate(query_refs):
-        rim = jnp.where(before == index, tail_rows(ref, rows // 4), rim)
+    rows, width = query_refs[0].shape[0] - RIM_ROWS, query_refs[0].shape[1]
+    rim = chosen_part(
+        [tail_rows(ref, rows // 4) for ref in query_refs], one_before(mask, lax.axis_index("sp"))
+    )
     lane = lax.broadcasted_iota(jnp.int32, (rows + RIM_ROWS, HEAD), 1)
     levels = jnp.zeros((rows + RIM_ROWS, HEAD), jnp.float32)
+    rim_parts = []
     for head in range(width // HEAD):
         columns = slice(head * HEAD, (head + 1) * HEAD)
-        query = jnp.concatenate([query_refs[mask][:, columns], rim[:, columns]], axis=0)
+        query = jnp.concatenate([query_refs[mask][:rows, columns], rim[:, columns]], axis=0)
         best, weight_sum, weighted = head_partial(query, keyval_refs)
-        out_ref[: rows + RIM_ROWS, columns] = (weighted / weight_sum).astype(jnp.bfloat16)
+        result = weighted / weight_sum
+        out_ref[:rows, columns] = result[:rows].astype(jnp.bfloat16)
+        rim_parts.append(result[rows:])
         levels = jnp.where(lane == head, best + jnp.log2(weight_sum), levels)
-    left, rim_left = levels[:rows].T[:STAT_ROWS], levels[rows:, :STAT_LANES]
-    for piece in range(3):
-        for part, place, size in ((left, piece * rows, rows), (rim_left, 3 * rows + piece * STAT_LANES, STAT_LANES)):
-            out_ref[rows + RIM_ROWS :, place : place + size] = part.astype(jnp.bfloat16)
+    left = levels[:rows].T[:RIM_ROWS]
+    rim_left = jnp.concatenate([levels[rows + 2 :], levels[rows : rows + 2]], axis=0)
+    row = lax.broadcasted_iota(jnp.int32, (RIM_ROWS, HEAD), 0)
+    for piece in range(width // HEAD):
+        here = jnp.where(row < 4, left, rim_left)
+        here = jnp.where(row < RIM_ROWS - 2, here, rim_parts[piece]).astype(jnp.bfloat16)
+        out_ref[rows:, piece * HEAD : (piece + 1) * HEAD] = here
         left = left - left.astype(jnp.bfloat16).astype(jnp.float32)
         rim_left = rim_left - rim_left.astype(jnp.bfloat16).astype(jnp.float32)
 
@@ -299,24 +363,12 @@
 def joined_heads(partial_refs, heads_ref):
     width = heads_ref.shape[1]
     rows = heads_ref.shape[0] - RIM_ROWS
-
-    def levels(start, size):
-        return [
-            sum(
-                ref[rows + RIM_ROWS :, start + piece * size : start + (piece + 1) * size].astype(jnp.float32)
-                for piece in range(3)
-            )
-            for ref in partial_refs
-        ]
-
-    filler = jnp.zeros((HEAD - STAT_ROWS, rows), jnp.float32)
-    columns = [
-        jnp.concatenate([share, filler], axis=0).T for share in shares_of(levels(0, rows))
-    ]
-    for cut, parts in (
-        (slice(0, rows), columns),
-        (slice(rows, rows + RIM_ROWS), shares_of(levels(3 * rows, STAT_LANES))),
-    ):
+    tails = [ref[rows:].astype(jnp.float32) for ref in partial_refs]
+    levels = [sum(tail[:, piece * HEAD : (piece + 1) * HEAD] for piece in range(3)) for tail in tails]
+    filler = jnp.zeros((HEAD - RIM_ROWS, rows), jnp.float32)
+    columns = [jnp.concatenate([share, filler], axis=0).T for share in shares_of(levels)]
+    rim_levels = [jnp.concatenate([level[-2:], level[:-2]], axis=0) for level in levels]
+    for cut, parts in ((slice(0, rows), columns), (slice(rows, None), shares_of(rim_levels))):
         for head in range(width // HEAD):
             lanes = slice(head * HEAD, (head + 1) * HEAD)
             heads_ref[cut, lanes] = sum(
@@ -347,11 +399,23 @@
         hidden_out[here] = normed(stream, pre_ref[...]).astype(jnp.bfloat16)
 
 
-def residual_rim_body(own_ref, other_ref, stream_ref, rim_ref, post_ref, pre_ref, stream_out, hidden_out, rim_out):
+def residual_rim_body(own_ref, other_ref, stream_ref, *refs):
+    *query_refs, post_ref, pre_ref, stream_out, hidden_out, rim_out = refs
     residual_body(own_ref, other_ref, stream_ref, post_ref, pre_ref, stream_out, hidden_out)
     half = stream_out.shape[0]
     mixed = own_ref[half:].astype(jnp.float32) + other_ref[half:].astype(jnp.float32)
-    stream = rim_ref[...].astype(jnp.float32) + normed(mixed, post_ref[...])
+    rows = query_refs[0].shape[0] - RIM_ROWS
+    wanted = one_before(0, lax.axis_index("sp"))
+    packed = chosen_part([ref[rows:].astype(jnp.float32) for ref in query_refs], wanted)
+    wide = RIM_ROWS // 2
+    last_two = [
+        jnp.concatenate([packed[row : row + 1] for row in range(index * wide, (index + 1) * wide)], axis=1)
+        for index in range(2)
+    ]
+    rim_rows = jnp.concatenate(
+        [jnp.zeros((RIM_ROWS - 2, mixed.shape[1]), jnp.float32), *last_two], axis=0
+    )
+    stream = rim_rows + normed(mixed, post_ref[...])
     rim = normed(stream, pre_ref[...])
     rim_out[...] = jnp.where(lax.axis_index("sp") == 0, 0.0, rim).astype(jnp.bfloat16)
 
@@ -389,7 +453,7 @@
     starts = [pl.multiple_of((place ^ mask) * quarter, quarter) for mask in LOCAL_ORDER]
     rows = jnp.concatenate([own_ref[...], other_ref[...], rim_ref[...]], axis=0)
     for weight_ref, ups in ((gate_ref, ups_gate), (value_ref, ups_value)):
-        product = dot_nt(rows, weight_ref[...])
+        product = dot32(rows, weight_ref[...])
         ups[:RIM_ROWS] = product[4 * quarter :].astype(jnp.bfloat16).astype(jnp.float32)
         for index, start in enumerate(starts):
             ups[pl.ds(start + RIM_ROWS, quarter)] = (
@@ -454,45 +518,62 @@
     swap = lambda value, axis, mask: swapped_mask(value, axis, mask)
     wide = shape_of(half, width)
 
+    query_first, pre_first, source_gain = fetched(query_first, row(pre_first), row(source_gain))
     own_target = jnp.concatenate([target, swap(target, "tp", 2)], axis=0)
     other_target = swap(own_target, "tp", 1)
-    queries, tail = launch(
+    queries = launch(
         query_body,
-        (shape_of(rows, head_width), shape_of(RIM_ROWS, width)),
+        shape_of(rows + RIM_ROWS, head_width),
         own_target,
         other_target,
         row(pre_first),
         query_first,
-        scratch=[pltpu.VMEM((rows, width), jnp.bfloat16)],
-    )
-    rim_target = shifted(tail, "sp", 1)
+        scratch=[pltpu.VMEM((rows, width), jnp.float32)],
+    )
     across = swap(queries, "sp", 2)
     query_blocks = (queries, swap(queries, "sp", 1), across, swap(across, "sp", 1))
 
-    span = source.shape[0] // CHUNKS
-    beside = swap(source, "tp", 1)
-    keyvals_first, keyvals_second = [], []
-    for chunk in range(CHUNKS):
-        cut = slice(chunk * span, (chunk + 1) * span)
-        across = swap(source[cut], "tp", 2)
-        chunk_rows, chunk_keyval = launch(
-            functools.partial(keyval_body, cut),
-            (shape_of(4 * span, width), shape_of(4 * span, keyval_width)),
-            source,
-            beside,
-            across,
-            swap(across, "tp", 1),
+    theirs = tuple(swap(weight, "tp", 1) for weight in (keyval_first, keyval_second))
+
+    def keyvals_of(piece):
+        size = piece.shape[0]
+        normed_piece, mine, other = launch(
+            keyval_body,
+            (shape_of(size, width), shape_of(size, keyval_width), shape_of(size, keyval_width)),
+            piece,
             row(source_gain),
             keyval_first,
+            theirs[0],
         )
-        keyvals_first.append(chunk_keyval)
-        here = launch(project_body, shape_of(4 * span, keyval_width), chunk_rows, keyval_second)
-        parts = [here]
+        return normed_piece, [mine, swap(other, "tp", 1)]
+
+    def later_keyvals(*pieces):
+        size = sum(piece.shape[0] for piece in pieces)
+        mine, other = launch(
+            keyval_later_body,
+            (shape_of(size, keyval_width),) * 2,
+            *pieces,
+            keyval_second,
+            theirs[1],
+        )
+        both = jnp.concatenate([mine, swap(other, "tp", 1)], axis=0)
+        parts = [both]
         for bit in reversed(range((sp_count - 1).bit_length())):
-            parts += [swap(part, "sp", 1 << bit) for part in parts]
-        keyvals_second += parts
-
-    packed = shape_of(rows + RIM_ROWS + STAT_ROWS, head_width)
+            parts += [swap(block, "sp", 1 << bit) for block in parts]
+        return parts
+
+    span = source.shape[0] // CHUNKS
+    normed_here, keyvals_first = keyvals_of(source)
+    keyvals_second = later_keyvals(normed_here)
+    normed_across = []
+    for chunk in range(CHUNKS):
+        across = swap(source[chunk * span : (chunk + 1) * span], "tp", 2)
+        normed_piece, made = keyvals_of(across)
+        normed_across.append(normed_piece)
+        keyvals_first += made
+    keyvals_second += later_keyvals(*normed_across)
+
+    packed = shape_of(rows + RIM_ROWS, head_width)
     partials = [None] * sp_count
     for mask in range(sp_count):
         partial = launch(
@@ -505,15 +586,15 @@
         keep = launch(project_body, shape_of(*send.shape), kept, weight)
         return (keep.astype(jnp.float32) + received.astype(jnp.float32)).astype(jnp.bfloat16)
 
-    def residual(own, post_gain, pre_gain, *streams):
+    def residual(own, post_gain, pre_gain, stream, *queries):
         other = swap(own, "tp", 2)
-        rims = tuple(shape_of(*stream.shape) for stream in streams[1:])
         return launch(
-            residual_rim_body if rims else residual_body,
-            (shape_of(half, width, jnp.float32), wide) + rims,
+            residual_rim_body if queries else residual_body,
+            (shape_of(half, width, jnp.float32), wide) + (shape_of(RIM_ROWS, width),) * bool(queries),
             own,
             other,
-            *streams,
+            stream,
+            *queries,
             row(post_gain),
             row(pre_gain),
         )
@@ -526,20 +607,24 @@
         scratch=[pltpu.VMEM((rows + RIM_ROWS, head_width), jnp.bfloat16)],
     )
     own = pair_sum(send, kept, out_first)
-    after_first, hidden, rim = residual(own, post_first, ffn_pre, own_target, rim_target)
+    after_first, hidden, rim = residual(own, post_first, ffn_pre, own_target, *query_blocks)
+    gate, value = launch(
+        turn_body, (shape_of(width, hidden_width),) * 2, w_gate.T, w_value.T, limit=14
+    )
     send, kept = launch(
         mixer_body,
         (wide, shape_of(half, hidden_width)),
         hidden,
         swap(hidden, "tp", 1),
         rim,
-        w_gate.T,
-        w_value.T,
+        gate,
+        value,
         conv_gate,
         conv_value,
         w_down,
         scratch=[pltpu.VMEM((rows + RIM_ROWS, hidden_width), jnp.float32)] * 2
         + [pltpu.VMEM((rows, hidden_width), jnp.bfloat16)],
+        limit=18,
     )
     own = pair_sum(send, kept, w_down)
     after_ffn, hidden = residual(own, ffn_post, pre_second, after_first)
@@ -552,7 +637,7 @@
         *keyvals_second,
         out_second,
         scratch=[pltpu.VMEM((rows, head_width), jnp.bfloat16)] * 2,
-        limit=32,
+        limit=20,
     )
     own = pair_sum(send, kept, out_second)
     return launch(
@@ -565,14 +650,16 @@
     )
 
 
-def fits(mesh, target, query_first, keyval_first):
+def fits(mesh, target, source, query_first, keyval_first):
     blocks, places = mesh.shape["sp"], mesh.shape["tp"]
     return (
         places == len(LOCAL_ORDER)
         and blocks == 4
         and target.shape[0] == mesh.shape["grp"] * blocks * HEAD
+        and source.shape[0] % (mesh.size * CHUNKS * HEAD) == 0
         and keyval_first.shape[1] == 2 * HEAD * places
-        and 3 * HEAD <= query_first.shape[1] // places <= STAT_ROWS * HEAD
+        and query_first.shape[1] == 4 * HEAD * places
+        and 2 * target.shape[1] == RIM_ROWS * query_first.shape[1] // places
     )
 
 
@@ -609,7 +696,7 @@
 
 
     def program(*arrays):
-        if not fits(mesh, arrays[0], arrays[4], arrays[5]):
+        if not fits(mesh, arrays[0], arrays[1], arrays[4], arrays[5]):
             return placed_body(per_device)(*arrays)
         return placed_body(per_device_paired)(*arrays)
 

time: 138 us -> 121 us (0.88)
  waiting for transfers between devices: 84.2 us -> 68.5 us
  starting transfers between devices: 30 us -> 26.2 us
    ppermute x27 -> x31, waiting for transfers between devices: 82.8 us -> 68.5 us  [swapped_mask(): lax.ppermute(block, axis, [(index, index ^ mask) for index in range(count)])]
    ppermute x1 -> x0, starting transfers between devices: 4.65 us -> none  [shifted(): lax.ppermute(value, axis, [(source, source + steps) for source in range(l...]
    ppermute x1 -> x0, waiting for transfers between devices: 1.4 us -> none  [shifted(): lax.ppermute(value, axis, [(source, source + steps) for source in range(l...]
    pallas_call x18 -> x20, Pallas kernels: 20.2 us -> 21.3 us  [launch(): pl.pallas_call(body, out_shape=outs, scratch_shapes=list(scratch), compil...]
    ppermute x27 -> x31, starting transfers between devices: 25.4 us -> 26.2 us  [swapped_mask(): lax.ppermute(block, axis, [(index, index ^ mask) for index in range(count)])]
  transfers between devices with their start and end apart: 28 -> 31, of which waited for: 17 -> 13; matrix products, arithmetic and copies ran while one was open for 0% -> 2% of each run, Pallas kernels for 7% -> 12%
where the time goes in v3:
time: 121 us
  waiting for transfers between devices  68.5 us (57%)
  starting transfers between devices  26.2 us (22%)
  Pallas kernels  21.5 us (18%)
  local copies, waits for them, and re-layouts  3.75 us (3%)
    ppermute x31, waiting for transfers between devices, swapped_mask(): lax.ppermute(block, axis, [(index, index ^ mask) for index in range(count)])  68.5 us
    ppermute x31, starting transfers between devices, swapped_mask(): lax.ppermute(block, axis, [(index, index ^ mask) for index in range(count)])  26.2 us
    pallas_call x20, Pallas kernels, launch(): pl.pallas_call(body, out_shape=outs, scratch_shapes=list(scratch), compil...  21.3 us
  transfers between devices with their start and end apart: 31, of which 13 were waited for; matrix products, arithmetic and copies ran while one was open for 2% of the time, Pallas kernels for 12%

profile of v3, /device:TPU:0, one launch (start us, length us, event | category | flops | bytes accessed | tf_op | source)
XLA Modules:
  0.0 120.7 jit_solution(11594382421486564392)
XLA Ops:
  0.0 3.0 %collective-permute-start = (bf16[32,2048]{1,0:T(8,128)(2,1)}, bf16[32,2048]{1,0:T(8,128)(2,1)S(1)}, u32[]{:S(2)}, u32[]{:S(2)}) collective-permute-start(bf16[32,2048]{1,0:T(8,128)(2,1)} %param.20), channel_id=1, source_target_pairs={{0,2},{1,3},{2,0},{3,1},{4,6},{5,7},{6,4},{7,5},{8,10},{9,11},{10,... | collective-permute-start | bytes 393224 | tf_op jit(solution)/shard_map/ppermute | solution.py:181
  3.0 1.3 %fusion = (bf16[128,2048]{1,0:T(8,128)(2,1)S(1)}, bf16[128,2048]{1,0:T(8,128)(2,1)S(1)}) fusion(bf16[256,2048]{1,0:T(8,128)(2,1)} %row_ref.1), kind=kLoop, calls=%fused_computation.9 | loop fusion | bytes 2097152 | tf_op jit(solution)/shard_map/slice | solution.py:570
  4.5 1.8 %collective-permute-start.7 = (bf16[128,2048]{1,0:T(8,128)(2,1)S(1)}, bf16[128,2048]{1,0:T(8,128)(2,1)S(1)}, u32[]{:S(2)}, u32[]{:S(2)}) collective-permute-start(bf16[128,2048]{1,0:T(8,128)(2,1)S(1)} %get-tuple-element.64), channel_id=1, source_target_pairs={{0,2},{1,3},{2,0},{3,1},{4,6},{5,7},{6,4},{7,5},{8,10},{9,11},{10,... | collective-permute-start | bytes 1572872 | tf_op jit(solution)/shard_map/ppermute | solution.py:181
  9.9 2.7 %collective-permute-start.3 = (bf16[136,512]{1,0:T(8,128)(2,1)S(1)}, bf16[136,512]{1,0:T(8,128)(2,1)S(1)}, u32[]{:S(2)}, u32[]{:S(2)}) collective-permute-start(bf16[136,512]{1,0:T(8,128)(2,1)S(1)} %shard_map.191.refs_0_), channel_id=1, source_target_pairs={{0,8},{4,12},{8,0},{12,4},{1,9},{5,13},{9,1},{13,5},{2,10},{6,14},... | collective-permute-start | bytes 417800 | tf_op jit(solution)/shard_map/ppermute | solution.py:181
  12.6 1.6 %collective-permute-start.2 = (bf16[136,512]{1,0:T(8,128)(2,1)S(1)}, bf16[136,512]{1,0:T(8,128)(2,1)S(1)}, u32[]{:S(2)}, u32[]{:S(2)}) collective-permute-start(bf16[136,512]{1,0:T(8,128)(2,1)S(1)} %shard_map.191.refs_0_), channel_id=1, source_target_pairs={{0,4},{4,0},{8,12},{12,8},{1,5},{5,1},{9,13},{13,9},{2,6},{6,2},{1... | collective-permute-start | bytes 417800 | tf_op jit(solution)/shard_map/ppermute | solution.py:181
  14.2 5.9 %collective-permute-done.3.refs_2_ = bf16[136,512]{1,0:T(8,128)(2,1)S(1)} collective-permute-done((bf16[136,512]{1,0:T(8,128)(2,1)S(1)}, bf16[136,512]{1,0:T(8,128)(2,1)S(1)}, u32[]{:S(2)}, u32[]{:S(2)}) %collective-permute-start.3) | collective-permute-done | bytes 139296 | tf_op jit(solution)/shard_map/ppermute | solution.py:181
  20.7 1.0 shard_map.192
  22.9 7.0 %collective-permute-done.7.row_ref = bf16[128,2048]{1,0:T(8,128)(2,1)S(1)} collective-permute-done((bf16[128,2048]{1,0:T(8,128)(2,1)S(1)}, bf16[128,2048]{1,0:T(8,128)(2,1)S(1)}, u32[]{:S(2)}, u32[]{:S(2)}) %collective-permute-start.7) | collective-permute-done | bytes 524320 | tf_op jit(solution)/shard_map/ppermute | solution.py:181
  30.7 1.2 %collective-permute-done.8.refs_7_ = bf16[128,256]{1,0:T(8,128)(2,1)S(1)} collective-permute-done((bf16[128,256]{1,0:T(8,128)(2,1)S(1)}, bf16[128,256]{1,0:T(8,128)(2,1)S(1)}, u32[]{:S(2)}, u32[]{:S(2)}) %collective-permute-start.8) | collective-permute-done | bytes 65568 | tf_op jit(solution)/shard_map/ppermute | solution.py:181
  31.9 1.2 shard_map.196
  33.0 1.6 %collective-permute-start.11 = (bf16[136,512]{1,0:T(8,128)(2,1)S(1)}, bf16[136,512]{1,0:T(8,128)(2,1)S(1)}, u32[]{:S(2)}, u32[]{:S(2)}) collective-permute-start(bf16[136,512]{1,0:T(8,128)(2,1)S(1)} %shard_map.196), channel_id=1, source_target_pairs={{0,4},{4,0},{8,12},{12,8},{1,5},{5,1},{9,13},{13,9},{2,6},{6,2},{1... | collective-permute-start | bytes 417800 | tf_op jit(solution)/shard_map/ppermute | solution.py:181
  34.7 1.1 shard_map.197
  35.8 2.6 %collective-permute-start.12 = (bf16[136,512]{1,0:T(8,128)(2,1)S(1)}, bf16[136,512]{1,0:T(8,128)(2,1)S(1)}, u32[]{:S(2)}, u32[]{:S(2)}) collective-permute-start(bf16[136,512]{1,0:T(8,128)(2,1)S(1)} %shard_map.197), channel_id=1, source_target_pairs={{0,8},{4,12},{8,0},{12,4},{1,9},{5,13},{9,1},{13,5},{2,10},{6,14},... | collective-permute-start | bytes 417800 | tf_op jit(solution)/shard_map/ppermute | solution.py:181
  38.5 1.1 shard_map.198
  39.9 1.1 shard_map.195.refs_0_
  41.1 8.1 %collective-permute-done.12.refs_2_ = bf16[136,512]{1,0:T(8,128)(2,1)S(1)} collective-permute-done((bf16[136,512]{1,0:T(8,128)(2,1)S(1)}, bf16[136,512]{1,0:T(8,128)(2,1)S(1)}, u32[]{:S(2)}, u32[]{:S(2)}) %collective-permute-start.12) | collective-permute-done | bytes 139296 | tf_op jit(solution)/shard_map/ppermute | solution.py:181
  51.8 1.0 collective-permute-start.15
  52.8 8.1 %collective-permute-done.15.other_ref = bf16[72,2048]{1,0:T(8,128)(2,1)S(1)} collective-permute-done((bf16[72,2048]{1,0:T(8,128)(2,1)S(1)}, bf16[72,2048]{1,0:T(8,128)(2,1)S(1)}, u32[]{:S(2)}, u32[]{:S(2)}) %collective-permute-start.15) | collective-permute-done | bytes 294944 | tf_op jit(solution)/shard_map/ppermute | solution.py:181
  61.3 1.7 %shard_map.202 = (bf16[2048,704]{1,0:T(8,128)(2,1)S(1)}, bf16[2048,704]{1,0:T(8,128)(2,1)S(1)}) custom-call(bf16[704,2048]{1,0:T(8,128)(2,1)S(1)} %bitcast.9, bf16[704,2048]{1,0:T(8,128)(2,1)S(1)} %bitcast.10), custom_call_target="tpu_custom_call" | custom-call | tf_op jit(solution)/shard_map/pallas_call | solution.py:207
  65.2 2.4 %shard_map.203 = (bf16[64,2048]{1,0:T(8,128)(2,1)S(1)}, bf16[64,704]{1,0:T(8,128)(2,1)S(1)}) custom-call(bf16[64,2048]{1,0:T(8,128)(2,1)S(1)} %get-tuple-element.45.own_ref, bf16[64,2048]{1,0:T(8,128)(2,1)S(1)} %collective-permute-done.16.other_ref, bf16[8,2048]{1,0:T(8,128)(2,1)S(1)} %get-tuple-element.46.rim_ref, ...), custom_call_target="tpu_custom_call" | custom-call | tf_op jit(solution)/shard_map/pallas_call | solution.py:207
  68.3 3.7 %collective-permute-start.22 = (bf16[512,256]{1,0:T(8,128)(2,1)S(1)}, bf16[512,256]{1,0:T(8,128)(2,1)S(1)}, u32[]{:S(2)}, u32[]{:S(2)}) collective-permute-start(bf16[512,256]{1,0:T(8,128)(2,1)S(1)} %constant_dynamic-update-slice_fusion.2.refs_3_), channel_id=1, source_target_pairs={{0,8},{4,12},{8,0},{12,4},{1,9},{5,13},{9,1},{13,5},{2,10},{6,14},... | collective-permute-start | bytes 786440 | tf_op jit(solution)/shard_map/ppermute | solution.py:181
  72.8 1.1 collective-permute-start.18
  73.9 1.8 %collective-permute-start.23 = (bf16[512,256]{1,0:T(8,128)(2,1)S(1)}, bf16[512,256]{1,0:T(8,128)(2,1)S(1)}, u32[]{:S(2)}, u32[]{:S(2)}) collective-permute-start(bf16[512,256]{1,0:T(8,128)(2,1)S(1)} %constant_dynamic-update-slice_fusion.2.refs_3_), channel_id=1, source_target_pairs={{0,4},{4,0},{8,12},{12,8},{1,5},{5,1},{9,13},{13,9},{2,6},{6,2},{1... | collective-permute-start | bytes 786440 | tf_op jit(solution)/shard_map/ppermute | solution.py:181
  75.9 14.6 %collective-permute-done.22.refs_4_ = bf16[512,256]{1,0:T(8,128)(2,1)S(1)} collective-permute-done((bf16[512,256]{1,0:T(8,128)(2,1)S(1)}, bf16[512,256]{1,0:T(8,128)(2,1)S(1)}, u32[]{:S(2)}, u32[]{:S(2)}) %collective-permute-start.22) | collective-permute-done | bytes 262176 | tf_op jit(solution)/shard_map/ppermute | solution.py:181
  90.5 5.0 %collective-permute-done.26.refs_8_ = bf16[512,256]{1,0:T(8,128)(2,1)S(1)} collective-permute-done((bf16[512,256]{1,0:T(8,128)(2,1)S(1)}, bf16[512,256]{1,0:T(8,128)(2,1)S(1)}, u32[]{:S(2)}, u32[]{:S(2)}) %collective-permute-start.26) | collective-permute-done | bytes 262176 | tf_op jit(solution)/shard_map/ppermute | solution.py:181
  95.9 2.9 %collective-permute-done.27.refs_9_ = bf16[512,256]{1,0:T(8,128)(2,1)S(1)} collective-permute-done((bf16[512,256]{1,0:T(8,128)(2,1)S(1)}, bf16[512,256]{1,0:T(8,128)(2,1)S(1)}, u32[]{:S(2)}, u32[]{:S(2)}) %collective-permute-start.27) | collective-permute-done | bytes 262176 | tf_op jit(solution)/shard_map/ppermute | solution.py:181
  98.8 5.6 %collective-permute-done.24.refs_6_ = bf16[512,256]{1,0:T(8,128)(2,1)S(1)} collective-permute-done((bf16[512,256]{1,0:T(8,128)(2,1)S(1)}, bf16[512,256]{1,0:T(8,128)(2,1)S(1)}, u32[]{:S(2)}, u32[]{:S(2)}) %collective-permute-start.24) | collective-permute-done | bytes 262176 | tf_op jit(solution)/shard_map/ppermute | solution.py:181
  104.4 4.1 %collective-permute-done.28.refs_10_ = bf16[512,256]{1,0:T(8,128)(2,1)S(1)} collective-permute-done((bf16[512,256]{1,0:T(8,128)(2,1)S(1)}, bf16[512,256]{1,0:T(8,128)(2,1)S(1)}, u32[]{:S(2)}, u32[]{:S(2)}) %collective-permute-start.28) | collective-permute-done | bytes 262176 | tf_op jit(solution)/shard_map/ppermute | solution.py:181
  108.5 4.0 %shard_map.208 = (bf16[64,2048]{1,0:T(8,128)(2,1)S(1)}, bf16[64,512]{1,0:T(8,128)(2,1)S(1)}) custom-call(bf16[64,2048]{1,0:T(8,128)(2,1)S(1)} %get-tuple-element.52.refs_0_, bf16[64,2048]{1,0:T(8,128)(2,1)S(1)} %collective-permute-done.19.refs_1_, bf16[2048,512]{1,0:T(8,128)(2,1)S(1)} %copy-done.9, ...), custom_call_target="tpu_custom_call" | custom-call | tf_op jit(solution)/shard_map/pallas_call | solution.py:207
  113.1 1.0 collective-permute-done.29
  114.3 1.1 collective-permute-start.30
  115.4 4.5 %collective-permute-done.30.other_ref = bf16[32,2048]{1,0:T(8,128)(2,1)S(1)} collective-permute-done((bf16[32,2048]{1,0:T(8,128)(2,1)S(1)}, bf16[32,2048]{1,0:T(8,128)(2,1)S(1)}, u32[]{:S(2)}, u32[]{:S(2)}) %collective-permute-start.30) | collective-permute-done | bytes 131104 | tf_op jit(solution)/shard_map/ppermute | solution.py:181
  (101 shorter events, 15.2 us)
Async XLA Ops:
  0.0 7.3 %collective-permute-start = (bf16[32,2048]{1,0:T(8,128)(2,1)}, bf16[32,2048]{1,0:T(8,128)(2,1)S(1)}, u32[]{:S(2)}, u32[]{:S(2)}) collective-permute-start(bf16[32,2048]{1,0:T(8,128)(2,1)} %param.20), channel_id=1, source_target_pairs={{0,2},{1,3},{2,0},{3,1},{4,6},{5,7},{6,4},{7,5},{8,10},{9,11},{10,... | collective-permute-start | bytes 393224 | tf_op jit(solution)/shard_map/ppermute | solution.py:181
  3.0 17.7 %collective-permute-start.5 = (bf16[2048,256]{1,0:T(8,128)(2,1)}, bf16[2048,256]{1,0:T(8,128)(2,1)S(1)}, u32[]{:S(2)}, u32[]{:S(2)}) collective-permute-start(bf16[2048,256]{1,0:T(8,128)(2,1)} %mine_ref.5), channel_id=1, source_target_pairs={{0,1},{1,0},{2,3},{3,2},{4,5},{5,4},{6,7},{7,6},{8,9},{9,8},{10,11... | collective-permute-start | bytes 3145736 | tf_op jit(solution)/shard_map/ppermute | solution.py:181
  4.3 17.5 %collective-permute-start.9 = (bf16[128,2048]{1,0:T(8,128)(2,1)S(1)}, bf16[128,2048]{1,0:T(8,128)(2,1)S(1)}, u32[]{:S(2)}, u32[]{:S(2)}) collective-permute-start(bf16[128,2048]{1,0:T(8,128)(2,1)S(1)} %get-tuple-element.63), channel_id=1, source_target_pairs={{0,2},{1,3},{2,0},{3,1},{4,6},{5,7},{6,4},{7,5},{8,10},{9,11},{10,... | collective-permute-start | bytes 1572872 | tf_op jit(solution)/shard_map/ppermute | solution.py:181
  4.5 25.4 %collective-permute-start.7 = (bf16[128,2048]{1,0:T(8,128)(2,1)S(1)}, bf16[128,2048]{1,0:T(8,128)(2,1)S(1)}, u32[]{:S(2)}, u32[]{:S(2)}) collective-permute-start(bf16[128,2048]{1,0:T(8,128)(2,1)S(1)} %get-tuple-element.64), channel_id=1, source_target_pairs={{0,2},{1,3},{2,0},{3,1},{4,6},{5,7},{6,4},{7,5},{8,10},{9,11},{10,... | collective-permute-start | bytes 1572872 | tf_op jit(solution)/shard_map/ppermute | solution.py:181
  7.3 1.7 %collective-permute-start.1 = (bf16[64,2048]{1,0:T(8,128)(2,1)S(1)}, bf16[64,2048]{1,0:T(8,128)(2,1)S(1)}, u32[]{:S(2)}, u32[]{:S(2)}) collective-permute-start(bf16[64,2048]{1,0:T(8,128)(2,1)S(1)} %constant_dynamic-update-slice_fusion.own_ref.stream_ref), channel_id=1, source_target_pairs={{0,1},{1,0},{2,3},{3,2},{4,5},{5,4},{6,7},{7,6},{8,9},{9,8},{10,11... | collective-permute-start | bytes 786440 | tf_op jit(solution)/shard_map/ppermute | solution.py:181
  9.9 10.1 %collective-permute-start.3 = (bf16[136,512]{1,0:T(8,128)(2,1)S(1)}, bf16[136,512]{1,0:T(8,128)(2,1)S(1)}, u32[]{:S(2)}, u32[]{:S(2)}) collective-permute-start(bf16[136,512]{1,0:T(8,128)(2,1)S(1)} %shard_map.191.refs_0_), channel_id=1, source_target_pairs={{0,8},{4,12},{8,0},{12,4},{1,9},{5,13},{9,1},{13,5},{2,10},{6,14},... | collective-permute-start | bytes 417800 | tf_op jit(solution)/shard_map/ppermute | solution.py:181
  12.6 18.0 %collective-permute-start.2 = (bf16[136,512]{1,0:T(8,128)(2,1)S(1)}, bf16[136,512]{1,0:T(8,128)(2,1)S(1)}, u32[]{:S(2)}, u32[]{:S(2)}) collective-permute-start(bf16[136,512]{1,0:T(8,128)(2,1)S(1)} %shard_map.191.refs_0_), channel_id=1, source_target_pairs={{0,4},{4,0},{8,12},{12,8},{1,5},{5,1},{9,13},{13,9},{2,6},{6,2},{1... | collective-permute-start | bytes 417800 | tf_op jit(solution)/shard_map/ppermute | solution.py:181
  20.1 10.6 %collective-permute-start.4 = (bf16[136,512]{1,0:T(8,128)(2,1)S(1)}, bf16[136,512]{1,0:T(8,128)(2,1)S(1)}, u32[]{:S(2)}, u32[]{:S(2)}) collective-permute-start(bf16[136,512]{1,0:T(8,128)(2,1)S(1)} %collective-permute-done.3.refs_2_), channel_id=1, source_target_pairs={{0,4},{4,0},{8,12},{12,8},{1,5},{5,1},{9,13},{13,9},{2,6},{6,2},{1... | collective-permute-start | bytes 417800 | tf_op jit(solution)/shard_map/ppermute | solution.py:181
  21.7 10.2 %collective-permute-start.6 = (bf16[256,256]{1,0:T(8,128)(2,1)S(1)}, bf16[256,256]{1,0:T(8,128)(2,1)S(1)}, u32[]{:S(2)}, u32[]{:S(2)}) collective-permute-start(bf16[256,256]{1,0:T(8,128)(2,1)S(1)} %get-tuple-element.38), channel_id=1, source_target_pairs={{0,1},{1,0},{2,3},{3,2},{4,5},{5,4},{6,7},{7,6},{8,9},{9,8},{10,11... | collective-permute-start | bytes 393224 | tf_op jit(solution)/shard_map/ppermute | solution.py:181
  22.4 8.3 %collective-permute-start.10 = (bf16[128,256]{1,0:T(8,128)(2,1)S(1)}, bf16[128,256]{1,0:T(8,128)(2,1)S(1)}, u32[]{:S(2)}, u32[]{:S(2)}) collective-permute-start(bf16[128,256]{1,0:T(8,128)(2,1)S(1)} %get-tuple-element.42), channel_id=1, source_target_pairs={{0,1},{1,0},{2,3},{3,2},{4,5},{5,4},{6,7},{7,6},{8,9},{9,8},{10,11... | collective-permute-start | bytes 196616 | tf_op jit(solution)/shard_map/ppermute | solution.py:181
  30.5 1.3 %collective-permute-start.8 = (bf16[128,256]{1,0:T(8,128)(2,1)S(1)}, bf16[128,256]{1,0:T(8,128)(2,1)S(1)}, u32[]{:S(2)}, u32[]{:S(2)}) collective-permute-start(bf16[128,256]{1,0:T(8,128)(2,1)S(1)} %get-tuple-element.40), channel_id=1, source_target_pairs={{0,1},{1,0},{2,3},{3,2},{4,5},{5,4},{6,7},{7,6},{8,9},{9,8},{10,11... | collective-permute-start | bytes 196616 | tf_op jit(solution)/shard_map/ppermute | solution.py:181
  33.0 8.0 %collective-permute-start.11 = (bf16[136,512]{1,0:T(8,128)(2,1)S(1)}, bf16[136,512]{1,0:T(8,128)(2,1)S(1)}, u32[]{:S(2)}, u32[]{:S(2)}) collective-permute-start(bf16[136,512]{1,0:T(8,128)(2,1)S(1)} %shard_map.196), channel_id=1, source_target_pairs={{0,4},{4,0},{8,12},{12,8},{1,5},{5,1},{9,13},{13,9},{2,6},{6,2},{1... | collective-permute-start | bytes 417800 | tf_op jit(solution)/shard_map/ppermute | solution.py:181
  35.8 13.3 %collective-permute-start.12 = (bf16[136,512]{1,0:T(8,128)(2,1)S(1)}, bf16[136,512]{1,0:T(8,128)(2,1)S(1)}, u32[]{:S(2)}, u32[]{:S(2)}) collective-permute-start(bf16[136,512]{1,0:T(8,128)(2,1)S(1)} %shard_map.197), channel_id=1, source_target_pairs={{0,8},{4,12},{8,0},{12,4},{1,9},{5,13},{9,1},{13,5},{2,10},{6,14},... | collective-permute-start | bytes 417800 | tf_op jit(solution)/shard_map/ppermute | solution.py:181
  39.6 9.5 %collective-permute-start.13 = (bf16[136,512]{1,0:T(8,128)(2,1)S(1)}, bf16[136,512]{1,0:T(8,128)(2,1)S(1)}, u32[]{:S(2)}, u32[]{:S(2)}) collective-permute-start(bf16[136,512]{1,0:T(8,128)(2,1)S(1)} %shard_map.198), channel_id=1, source_target_pairs={{0,12},{4,8},{8,4},{12,0},{1,13},{5,9},{9,5},{13,1},{2,14},{6,10},... | collective-permute-start | bytes 417800 | tf_op jit(solution)/shard_map/ppermute | solution.py:181
  50.0 1.6 %collective-permute-start.14 = (bf16[72,2048]{1,0:T(8,128)(2,1)S(1)}, bf16[72,2048]{1,0:T(8,128)(2,1)S(1)}, u32[]{:S(2)}, u32[]{:S(2)}) collective-permute-start(bf16[72,2048]{1,0:T(8,128)(2,1)S(1)} %get-tuple-element.44), channel_id=1, source_target_pairs={{0,1},{1,0},{2,3},{3,2},{4,5},{5,4},{6,7},{7,6},{8,9},{9,8},{10,11... | collective-permute-start | bytes 884744 | tf_op jit(solution)/shard_map/ppermute | solution.py:181
  50.1 12.9 %collective-permute-start.20 = (bf16[2048,256]{1,0:T(8,128)(2,1)S(1)}, bf16[2048,256]{1,0:T(8,128)(2,1)S(1)}, u32[]{:S(2)}, u32[]{:S(2)}) collective-permute-start(bf16[2048,256]{1,0:T(8,128)(2,1)S(1)} %copy-done.4), channel_id=1, source_target_pairs={{0,1},{1,0},{2,3},{3,2},{4,5},{5,4},{6,7},{7,6},{8,9},{9,8},{10,11... | collective-permute-start | bytes 3145736 | tf_op jit(solution)/shard_map/ppermute | solution.py:181
  51.8 9.1 %collective-permute-start.15 = (bf16[72,2048]{1,0:T(8,128)(2,1)S(1)}, bf16[72,2048]{1,0:T(8,128)(2,1)S(1)}, u32[]{:S(2)}, u32[]{:S(2)}) collective-permute-start(bf16[72,2048]{1,0:T(8,128)(2,1)S(1)} %add_convert_fusion.own_ref), channel_id=1, source_target_pairs={{0,2},{1,3},{2,0},{3,1},{4,6},{5,7},{6,4},{7,5},{8,10},{9,11},{10,... | collective-permute-start | bytes 884744 | tf_op jit(solution)/shard_map/ppermute | solution.py:181
  61.2 4.0 %collective-permute-start.16 = (bf16[64,2048]{1,0:T(8,128)(2,1)S(1)}, bf16[64,2048]{1,0:T(8,128)(2,1)S(1)}, u32[]{:S(2)}, u32[]{:S(2)}) collective-permute-start(bf16[64,2048]{1,0:T(8,128)(2,1)S(1)} %get-tuple-element.45.own_ref), channel_id=1, source_target_pairs={{0,1},{1,0},{2,3},{3,2},{4,5},{5,4},{6,7},{7,6},{8,9},{9,8},{10,11... | collective-permute-start | bytes 786440 | tf_op jit(solution)/shard_map/ppermute | solution.py:181
  63.8 4.4 %collective-permute-start.21 = (bf16[256,256]{1,0:T(8,128)(2,1)S(1)}, bf16[256,256]{1,0:T(8,128)(2,1)S(1)}, u32[]{:S(2)}, u32[]{:S(2)}) collective-permute-start(bf16[256,256]{1,0:T(8,128)(2,1)S(1)} %get-tuple-element.55), channel_id=1, source_target_pairs={{0,1},{1,0},{2,3},{3,2},{4,5},{5,4},{6,7},{7,6},{8,9},{9,8},{10,11... | collective-permute-start | bytes 393224 | tf_op jit(solution)/shard_map/ppermute | solution.py:181
  65.1 6.9 %collective-permute-start.25 = (bf16[256,256]{1,0:T(8,128)(2,1)S(1)}, bf16[256,256]{1,0:T(8,128)(2,1)S(1)}, u32[]{:S(2)}, u32[]{:S(2)}) collective-permute-start(bf16[256,256]{1,0:T(8,128)(2,1)S(1)} %get-tuple-element.59), channel_id=1, source_target_pairs={{0,1},{1,0},{2,3},{3,2},{4,5},{5,4},{6,7},{7,6},{8,9},{9,8},{10,11... | collective-permute-start | bytes 393224 | tf_op jit(solution)/shard_map/ppermute | solution.py:181
  67.7 5.1 %collective-permute-start.17 = (bf16[64,2048]{1,0:T(8,128)(2,1)S(1)}, bf16[64,2048]{1,0:T(8,128)(2,1)S(1)}, u32[]{:S(2)}, u32[]{:S(2)}) collective-permute-start(bf16[64,2048]{1,0:T(8,128)(2,1)S(1)} %get-tuple-element.50), channel_id=1, source_target_pairs={{0,1},{1,0},{2,3},{3,2},{4,5},{5,4},{6,7},{7,6},{8,9},{9,8},{10,11... | collective-permute-start | bytes 786440 | tf_op jit(solution)/shard_map/ppermute | solution.py:181
  68.2 40.3 %copy-start.9 = (bf16[2048,512]{1,0:T(8,128)(2,1)S(1)}, bf16[2048,512]{1,0:T(8,128)(2,1)}, u32[]{:S(2)}) copy-start(bf16[2048,512]{1,0:T(8,128)(2,1)} %refs_2_.3) | copy-start | bytes 6291460
  68.3 22.2 %collective-permute-start.22 = (bf16[512,256]{1,0:T(8,128)(2,1)S(1)}, bf16[512,256]{1,0:T(8,128)(2,1)S(1)}, u32[]{:S(2)}, u32[]{:S(2)}) collective-permute-start(bf16[512,256]{1,0:T(8,128)(2,1)S(1)} %constant_dynamic-update-slice_fusion.2.refs_3_), channel_id=1, source_target_pairs={{0,8},{4,12},{8,0},{12,4},{1,9},{5,13},{9,1},{13,5},{2,10},{6,14},... | collective-permute-start | bytes 786440 | tf_op jit(solution)/shard_map/ppermute | solution.py:181
  72.0 23.4 %collective-permute-start.26 = (bf16[512,256]{1,0:T(8,128)(2,1)S(1)}, bf16[512,256]{1,0:T(8,128)(2,1)S(1)}, u32[]{:S(2)}, u32[]{:S(2)}) collective-permute-start(bf16[512,256]{1,0:T(8,128)(2,1)S(1)} %constant_dynamic-update-slice_fusion.4.refs_7_), channel_id=1, source_target_pairs={{0,8},{4,12},{8,0},{12,4},{1,9},{5,13},{9,1},{13,5},{2,10},{6,14},... | collective-permute-start | bytes 786440 | tf_op jit(solution)/shard_map/ppermute | solution.py:181
  72.8 22.6 %collective-permute-start.18 = (bf16[64,2048]{1,0:T(8,128)(2,1)S(1)}, bf16[64,2048]{1,0:T(8,128)(2,1)S(1)}, u32[]{:S(2)}, u32[]{:S(2)}) collective-permute-start(bf16[64,2048]{1,0:T(8,128)(2,1)S(1)} %add_convert_fusion.2.own_ref), channel_id=1, source_target_pairs={{0,2},{1,3},{2,0},{3,1},{4,6},{5,7},{6,4},{7,5},{8,10},{9,11},{10,... | collective-permute-start | bytes 786440 | tf_op jit(solution)/shard_map/ppermute | solution.py:181
  73.9 22.0 %collective-permute-start.23 = (bf16[512,256]{1,0:T(8,128)(2,1)S(1)}, bf16[512,256]{1,0:T(8,128)(2,1)S(1)}, u32[]{:S(2)}, u32[]{:S(2)}) collective-permute-start(bf16[512,256]{1,0:T(8,128)(2,1)S(1)} %constant_dynamic-update-slice_fusion.2.refs_3_), channel_id=1, source_target_pairs={{0,4},{4,0},{8,12},{12,8},{1,5},{5,1},{9,13},{13,9},{2,6},{6,2},{1... | collective-permute-start | bytes 786440 | tf_op jit(solution)/shard_map/ppermute | solution.py:181
  75.7 23.1 %collective-permute-start.27 = (bf16[512,256]{1,0:T(8,128)(2,1)S(1)}, bf16[512,256]{1,0:T(8,128)(2,1)S(1)}, u32[]{:S(2)}, u32[]{:S(2)}) collective-permute-start(bf16[512,256]{1,0:T(8,128)(2,1)S(1)} %constant_dynamic-update-slice_fusion.4.refs_7_), channel_id=1, source_target_pairs={{0,4},{4,0},{8,12},{12,8},{1,5},{5,1},{9,13},{13,9},{2,6},{6,2},{1... | collective-permute-start | bytes 786440 | tf_op jit(solution)/shard_map/ppermute | solution.py:181
  90.5 13.9 %collective-permute-start.24 = (bf16[512,256]{1,0:T(8,128)(2,1)S(1)}, bf16[512,256]{1,0:T(8,128)(2,1)S(1)}, u32[]{:S(2)}, u32[]{:S(2)}) collective-permute-start(bf16[512,256]{1,0:T(8,128)(2,1)S(1)} %collective-permute-done.22.refs_4_), channel_id=1, source_target_pairs={{0,4},{4,0},{8,12},{12,8},{1,5},{5,1},{9,13},{13,9},{2,6},{6,2},{1... | collective-permute-start | bytes 786440 | tf_op jit(solution)/shard_map/ppermute | solution.py:181
  95.4 13.1 %collective-permute-start.28 = (bf16[512,256]{1,0:T(8,128)(2,1)S(1)}, bf16[512,256]{1,0:T(8,128)(2,1)S(1)}, u32[]{:S(2)}, u32[]{:S(2)}) collective-permute-start(bf16[512,256]{1,0:T(8,128)(2,1)S(1)} %collective-permute-done.26.refs_8_), channel_id=1, source_target_pairs={{0,4},{4,0},{8,12},{12,8},{1,5},{5,1},{9,13},{13,9},{2,6},{6,2},{1... | collective-permute-start | bytes 786440 | tf_op jit(solution)/shard_map/ppermute | solution.py:181
  95.8 12.7 %collective-permute-start.19 = (bf16[64,2048]{1,0:T(8,128)(2,1)S(1)}, bf16[64,2048]{1,0:T(8,128)(2,1)S(1)}, u32[]{:S(2)}, u32[]{:S(2)}) collective-permute-start(bf16[64,2048]{1,0:T(8,128)(2,1)S(1)} %get-tuple-element.52.refs_0_), channel_id=1, source_target_pairs={{0,1},{1,0},{2,3},{3,2},{4,5},{5,4},{6,7},{7,6},{8,9},{9,8},{10,11... | collective-permute-start | bytes 786440 | tf_op jit(solution)/shard_map/ppermute | solution.py:181
  112.6 1.6 %collective-permute-start.29 = (bf16[64,2048]{1,0:T(8,128)(2,1)S(1)}, bf16[64,2048]{1,0:T(8,128)(2,1)S(1)}, u32[]{:S(2)}, u32[]{:S(2)}) collective-permute-start(bf16[64,2048]{1,0:T(8,128)(2,1)S(1)} %get-tuple-element.61), channel_id=1, source_target_pairs={{0,1},{1,0},{2,3},{3,2},{4,5},{5,4},{6,7},{7,6},{8,9},{9,8},{10,11... | collective-permute-start | bytes 786440 | tf_op jit(solution)/shard_map/ppermute | solution.py:181
  114.3 5.6 %collective-permute-start.30 = (bf16[32,2048]{1,0:T(8,128)(2,1)S(1)}, bf16[32,2048]{1,0:T(8,128)(2,1)S(1)}, u32[]{:S(2)}, u32[]{:S(2)}) collective-permute-start(bf16[32,2048]{1,0:T(8,128)(2,1)S(1)} %get-tuple-element.65), channel_id=1, source_target_pairs={{0,2},{1,3},{2,0},{3,1},{4,6},{5,7},{6,4},{7,5},{8,10},{9,11},{10,... | collective-permute-start | bytes 393224 | tf_op jit(solution)/shard_map/ppermute | solution.py:181
  (18 other events, 250.1 us)
